TPU v7x, 32 devices: a whole 2x2x4 slice. The times are simulated.
32 devices in a mesh: grp: 1, sp: 16 (over z, y, core), tp: 2 (over x).
Axes of the slice: x: 2, y: 2, z: 4, core: 2. Of those that a mesh axis runs over, the one named last changes fastest.
Arguments:
- residual_in: bfloat16 [2048, 2048], P(('grp', 'sp'), 'tp'), may hold values from -16 to 16
- query_pre: bfloat16 [2048, 512], P(('grp', 'sp'), 'tp'), may hold values from -6 to 6
- forget_pre: bfloat16 [2048, 512], P(('grp', 'sp'), 'tp'), may hold values from -9 to 9
- value_pre: bfloat16 [2048, 512], P(('grp', 'sp'), 'tp'), may hold values from -6 to 6
- gate_pre: bfloat16 [2048, 512], P(('grp', 'sp'), 'tp'), may hold values from -6 to 6
- floor_gap: float32 [512], P('tp'), may hold values from 0 to 1, as said below
- head_gain: float32 [64], replicated, may hold values from 0.1 to 1.9
- out_weight: bfloat16 [512, 2048], P(None, 'tp'), may hold values from -0.25 to 0.25
- norm_gain: float32 [2048], P('tp'), may hold values from 0.1 to 1.9
- value_weight: bfloat16 [2048, 5632], P('sp', 'tp'), may hold values from -0.125 to 0.125
- gate_weight: bfloat16 [2048, 5632], P('sp', 'tp'), may hold values from -0.125 to 0.125
- value_taps: float32 [3, 5632], P(None, 'tp'), may hold values from -3 to 3
- gate_taps: float32 [3, 5632], P(None, 'tp'), may hold values from -3 to 3
- down_weight: bfloat16 [5632, 2048], P('tp', 'sp'), may hold values from -0.078125 to 0.078125
Outputs:
- mixed: bfloat16 [2048, 2048], P(('grp', 'sp'), 'tp')
Inputs may be any that keep to these rules, and one draw needn't show every extreme that they name: `floor_gap`: each channel's value lies strictly between 0 and 1.
All inputs are finite; a program needn't handle non-finite values.
Results may differ from a plain program's by a relative error of at most 0.0085.
Values may be sent and summed in bfloat16 or wider, within the bound.
A program may use at most 128 MiB of HBM per device.

v0:
```python
import jax
import jax.numpy as jnp
from jax import lax
from jax.sharding import PartitionSpec as P

D = 2048
DK = 64
DV = 64
BLOCK = 64


epsilon = 1e-06
highest_precision = lax.Precision.HIGHEST


def shifted(array, axis, by):
    length = lax.axis_size(axis)
    pairs = [(i, i + by) for i in range(length) if 0 <= i + by < length]
    return lax.ppermute(array, axis, pairs)


def split_heads(matrix, head_count):
    return matrix.reshape(matrix.shape[0], head_count, -1).transpose(1, 0, 2)


def recurrence(query_rows, gate_keys, values, log_decay, block_size, start_state):
    head_count, seq_length, key_width = query_rows.shape
    block_count = seq_length // block_size

    def to_blocks(tensor):
        return tensor.reshape(head_count, block_count, block_size, tensor.shape[-1]).transpose(
            1, 0, 2, 3
        )

    causal = jnp.tril(jnp.ones((block_size, block_size), dtype=bool))

    def advance(current_state, inputs):
        block_queries, block_keys, block_values, decay_block = inputs
        running_state = jnp.cumsum(decay_block, axis=1)
        carried_state = jnp.einsum(
            "pen,pnd->ped",
            block_queries * jnp.exp(running_state),
            current_state,
            precision=highest_precision,
        )
        spread = jnp.where(
            causal[None, :, :, None],
            running_state[:, :, None, :] - running_state[:, None, :, :],
            -jnp.inf,
        )
        scores = jnp.einsum(
            "htk,hsk,htsk->hts",
            block_queries,
            block_keys,
            jnp.exp(spread),
            precision=highest_precision,
        )
        inner = jnp.einsum("hts,hsv->htv", scores, block_values, precision=highest_precision)
        ending_state = running_state[:, -1, :]
        fresh_update = jnp.einsum(
            "bia,big->bag",
            block_keys * jnp.exp(ending_state[:, None, :] - running_state),
            block_values,
            precision=highest_precision,
        )
        return (
            jnp.exp(ending_state)[:, :, None] * current_state + fresh_update,
            carried_state + inner,
        )

    final_state, outputs = lax.scan(
        advance,
        start_state,
        (to_blocks(query_rows), to_blocks(gate_keys), to_blocks(values), to_blocks(log_decay)),
    )
    return (
        final_state,
        outputs.transpose(1, 0, 2, 3).reshape(head_count, seq_length, values.shape[-1]),
    )


def mixer_inputs(query_pre, forget_pre, value_pre, floor_gap, head_count):
    gate_keys = floor_gap * jax.nn.sigmoid(-forget_pre.astype(jnp.float32))
    log_decay = jnp.log1p(-gate_keys)
    query_rows = jax.nn.silu(query_pre.astype(jnp.float32))
    return (
        split_heads(query_rows, head_count),
        split_heads(gate_keys, head_count),
        split_heads(value_pre.astype(jnp.float32), head_count),
        split_heads(log_decay, head_count),
    )


def head_output(recurrent, head_gain, gate_pre):
    ordered = recurrent.transpose(1, 0, 2)
    scaled = (
        ordered
        * lax.rsqrt(jnp.mean(ordered * ordered, axis=-1, keepdims=True) + epsilon)
        * head_gain
    )
    gating = jax.nn.silu(gate_pre.astype(jnp.float32)).reshape(ordered.shape)
    return (scaled * gating).reshape(ordered.shape[0], -1).astype(jnp.bfloat16)


def causal_taps(padded, taps, row_count):
    return (
        taps[0] * padded[0:row_count]
        + taps[1] * padded[1 : row_count + 1]
        + taps[2] * padded[2 : row_count + 2]
    )


def on_device(
    residual_in,
    query_pre,
    forget_pre,
    value_pre,
    gate_pre,
    floor_gap,
    head_gain,
    out_weight,
    norm_gain,
    value_weight,
    gate_weight,
    value_taps,
    gate_taps,
    down_weight,
):
    row_count = residual_in.shape[0]
    local_heads = floor_gap.shape[0] // DK
    query_rows, gate_keys, values, log_decay = mixer_inputs(
        query_pre, forget_pre, value_pre, floor_gap, local_heads
    )
    zero_state = jnp.zeros((local_heads, DK, DV), jnp.float32)
    final_state, recurrent = recurrence(query_rows, gate_keys, values, log_decay, BLOCK, zero_state)
    decay_from_start = jnp.cumsum(log_decay, axis=1)
    total_decay = jnp.exp(decay_from_start[:, -1, :])

    def pass_along(turn_index, incoming):
        return shifted(total_decay[:, :, None] * incoming + final_state, "sp", 1)

    entering_state = lax.fori_loop(0, lax.axis_size("sp") - 1, pass_along, zero_state)
    recurrent = recurrent + jnp.einsum(
        "pen,pnd->ped",
        query_rows * jnp.exp(decay_from_start),
        entering_state,
        precision=highest_precision,
    )
    head_out = head_output(recurrent, head_gain, gate_pre)
    projected = jnp.dot(
        lax.all_gather(head_out, "tp", axis=1, tiled=True),
        out_weight,
        preferred_element_type=jnp.float32,
    )
    stream = residual_in.astype(jnp.float32) + projected
    squares = lax.psum(jnp.sum(stream * stream, axis=1), "tp")
    normed_part = (stream * lax.rsqrt(squares / D + epsilon)[:, None] * norm_gain).astype(
        jnp.bfloat16
    )
    normed = lax.all_gather(normed_part, "tp", axis=1, tiled=True)
    sum_value = jnp.dot(
        normed,
        lax.all_gather(value_weight, "sp", axis=0, tiled=True),
        preferred_element_type=jnp.float32,
    )
    sum_gate = jnp.dot(
        normed,
        lax.all_gather(gate_weight, "sp", axis=0, tiled=True),
        preferred_element_type=jnp.float32,
    )
    up_value = sum_value.astype(jnp.bfloat16)
    up_gate = sum_gate.astype(jnp.bfloat16)
    hidden_width = up_value.shape[1]
    tail_rows = jnp.concatenate([up_value[row_count - 2 :], up_gate[row_count - 2 :]], axis=1)
    before = shifted(tail_rows, "sp", 1)
    padded_value = jnp.concatenate([before[:, :hidden_width], up_value], axis=0).astype(jnp.float32)
    padded_gate = jnp.concatenate([before[:, hidden_width:], up_gate], axis=0).astype(jnp.float32)
    conv_value = causal_taps(padded_value, value_taps, row_count)
    conv_gate = causal_taps(padded_gate, gate_taps, row_count)
    hidden = (jax.nn.silu(conv_gate) * conv_value).astype(jnp.bfloat16)
    terms = jnp.dot(
        hidden,
        lax.all_gather(down_weight, "sp", axis=1, tiled=True),
        preferred_element_type=jnp.float32,
    )
    down_part = lax.psum_scatter(
        terms.astype(jnp.bfloat16), "tp", scatter_dimension=1, tiled=True
    ).astype(jnp.float32)
    return (stream + down_part).astype(jnp.bfloat16)


def solution(mesh):
    return jax.shard_map(
        on_device,
        mesh=mesh,
        in_specs=(
            P(("grp", "sp"), "tp"),
            P(("grp", "sp"), "tp"),
            P(("grp", "sp"), "tp"),
            P(("grp", "sp"), "tp"),
            P(("grp", "sp"), "tp"),
            P("tp"),
            P(),
            P(None, "tp"),
            P("tp"),
            P("sp", "tp"),
            P("sp", "tp"),
            P(None, "tp"),
            P(None, "tp"),
            P("tp", "sp"),
        ),
        out_specs=P(("grp", "sp"), "tp"),
        check_vma=False,
    )
```

profile of v0, /device:TPU:0, one launch (start us, length us, event | category | flops | bytes accessed | tf_op | source)
XLA Modules:
  0.0 344.4 jit_solution(7182356617258133843)
XLA Ops:
  10.6 42.8 %while.24 = (s32[]{:T(128)}, f32[4,64,64]{2,1,0:T(8,128)S(1)}, f32[2,4,64,64]{3,2,1,0:T(8,128)}, f32[2,4,64,64]{2,0,3,1:T(2,128)S(1)}, f32[2,4,64,64]{2,0,3,1:T(...) while((s32[]{:T(128)}, f32[4,64,64]{2,1,0:T(8,128)S(1)}, ...), condition=%wide.region_2.3_spmd.clone, body=%wide.region_0.2_spmd.clone.sunk | while | flops 44142592 | bytes 19217028 | solution.py:71
  11.0 4.3 %select_exponential_fusion.2 = f32[4,64,64,64]{3,2,1,0:T(8,128)} fusion(f32[4,64,64]{2,1,0:T(8,128)S(1)} %reduce_window_sum.25, pred[64,64]{1,0:T(8,128)(4,1)S(1)} %iota_compare_fusion.2), kind=kLoop, calls=%fused_computation.4.clone.1 | loop fusion | flops 2097152 | bytes 4263936 | tf_op jit(solution)/shard_map/while/body/eval_jaxpr/exp | solution.py:55
  15.3 9.2 %copy.62 = f32[4,64,64,64]{1,2,3,0:T(8,128)} copy(f32[4,64,64,64]{3,2,1,0:T(8,128)} %select_exponential_fusion.2) | data formatting | bytes 8388608 | tf_op jit(solution)/shard_map/while
  24.9 5.2 %fusion.63 = f32[4,64,64]{1,2,0:T(8,128)S(1)} fusion(f32[4,64,64,64]{1,2,3,0:T(8,128)} %copy.62, f32[4,64,64]{2,1,0:T(8,128)S(1)} %copy.63, f32[4,64,64]{2,1,0:T(8,128)S(1)} %bitcast.102), kind=kLoop, calls=%fused_computation.3.clone.1 | loop fusion | flops 3129344 | bytes 4390912 | tf_op jit(solution)/shard_map/while/body/eval_jaxpr/htk,hsk,htsk->hts/dot_general | solution.py:51
  32.5 4.3 %select_exponential_fusion.2 = f32[4,64,64,64]{3,2,1,0:T(8,128)} fusion(f32[4,64,64]{2,1,0:T(8,128)S(1)} %reduce_window_sum.25, pred[64,64]{1,0:T(8,128)(4,1)S(1)} %iota_compare_fusion.2), kind=kLoop, calls=%fused_computation.4.clone.1 | loop fusion | flops 2097152 | bytes 4263936 | tf_op jit(solution)/shard_map/while/body/eval_jaxpr/exp | solution.py:55
  36.8 9.1 %copy.62 = f32[4,64,64,64]{1,2,3,0:T(8,128)} copy(f32[4,64,64,64]{3,2,1,0:T(8,128)} %select_exponential_fusion.2) | data formatting | bytes 8388608 | tf_op jit(solution)/shard_map/while
  46.3 5.2 %fusion.63 = f32[4,64,64]{1,2,0:T(8,128)S(1)} fusion(f32[4,64,64,64]{1,2,3,0:T(8,128)} %copy.62, f32[4,64,64]{2,1,0:T(8,128)S(1)} %copy.63, f32[4,64,64]{2,1,0:T(8,128)S(1)} %bitcast.102), kind=kLoop, calls=%fused_computation.3.clone.1 | loop fusion | flops 3129344 | bytes 4390912 | tf_op jit(solution)/shard_map/while/body/eval_jaxpr/htk,hsk,htsk->hts/dot_general | solution.py:51
  54.9 128.5 %while.23 = (s32[]{:T(128)}, f32[4,64,64]{2,1,0:T(8,128)S(1)}, f32[4,64]{1,0:T(4,128)S(1)}, f32[4,64,64]{2,1,0:T(8,128)S(1)}, s32[]{:T(128)}) while((s32[]{:T(128)}, f32[4,64,64]{2,1,0:T(8,128)S(1)}, f32[4,64]{1,0:T(4,128)S(1)}, f32[4,64,64]{2,1,0:T(8,128)S(1)}, s32[]{:T(128)}) %tuple.69), condition=%wide.region_5.6_spmd, body=%wide.region_4.5_spmd.sunk | while | flops 32770 | bytes 459877 | solution.py:142
  55.0 2.4 collective-permute-start
  58.5 8.4 %collective-permute-start = (f32[4,64,64]{2,1,0:T(8,128)S(1)}, f32[4,64,64]{2,1,0:T(8,128)S(1)}, u32[]{:S(2)}, u32[]{:S(2)}) collective-permute-start(f32[4,64,64]{2,1,0:T(8,128)S(1)} %multiply_add_fusion.2), channel_id=1, source_target_pairs={{0,2},{2,4},{4,6},{6,8},{8,10},{10,12},{12,14},{14,16},{16,18},{18... | collective-permute-start | bytes 196616 | tf_op jit(solution)/shard_map/while/body/eval_jaxpr/ppermute | solution.py:19
  67.9 8.2 %collective-permute-start = (f32[4,64,64]{2,1,0:T(8,128)S(1)}, f32[4,64,64]{2,1,0:T(8,128)S(1)}, u32[]{:S(2)}, u32[]{:S(2)}) collective-permute-start(f32[4,64,64]{2,1,0:T(8,128)S(1)} %multiply_add_fusion.2), channel_id=1, source_target_pairs={{0,2},{2,4},{4,6},{6,8},{8,10},{10,12},{12,14},{14,16},{16,18},{18... | collective-permute-start | bytes 196616 | tf_op jit(solution)/shard_map/while/body/eval_jaxpr/ppermute | solution.py:19
  77.2 8.2 %collective-permute-start = (f32[4,64,64]{2,1,0:T(8,128)S(1)}, f32[4,64,64]{2,1,0:T(8,128)S(1)}, u32[]{:S(2)}, u32[]{:S(2)}) collective-permute-start(f32[4,64,64]{2,1,0:T(8,128)S(1)} %multiply_add_fusion.2), channel_id=1, source_target_pairs={{0,2},{2,4},{4,6},{6,8},{8,10},{10,12},{12,14},{14,16},{16,18},{18... | collective-permute-start | bytes 196616 | tf_op jit(solution)/shard_map/while/body/eval_jaxpr/ppermute | solution.py:19
  86.6 5.4 %collective-permute-start = (f32[4,64,64]{2,1,0:T(8,128)S(1)}, f32[4,64,64]{2,1,0:T(8,128)S(1)}, u32[]{:S(2)}, u32[]{:S(2)}) collective-permute-start(f32[4,64,64]{2,1,0:T(8,128)S(1)} %multiply_add_fusion.2), channel_id=1, source_target_pairs={{0,2},{2,4},{4,6},{6,8},{8,10},{10,12},{12,14},{14,16},{16,18},{18... | collective-permute-start | bytes 196616 | tf_op jit(solution)/shard_map/while/body/eval_jaxpr/ppermute | solution.py:19
  93.0 5.3 %collective-permute-start = (f32[4,64,64]{2,1,0:T(8,128)S(1)}, f32[4,64,64]{2,1,0:T(8,128)S(1)}, u32[]{:S(2)}, u32[]{:S(2)}) collective-permute-start(f32[4,64,64]{2,1,0:T(8,128)S(1)} %multiply_add_fusion.2), channel_id=1, source_target_pairs={{0,2},{2,4},{4,6},{6,8},{8,10},{10,12},{12,14},{14,16},{16,18},{18... | collective-permute-start | bytes 196616 | tf_op jit(solution)/shard_map/while/body/eval_jaxpr/ppermute | solution.py:19
  99.4 6.6 %collective-permute-start = (f32[4,64,64]{2,1,0:T(8,128)S(1)}, f32[4,64,64]{2,1,0:T(8,128)S(1)}, u32[]{:S(2)}, u32[]{:S(2)}) collective-permute-start(f32[4,64,64]{2,1,0:T(8,128)S(1)} %multiply_add_fusion.2), channel_id=1, source_target_pairs={{0,2},{2,4},{4,6},{6,8},{8,10},{10,12},{12,14},{14,16},{16,18},{18... | collective-permute-start | bytes 196616 | tf_op jit(solution)/shard_map/while/body/eval_jaxpr/ppermute | solution.py:19
  107.1 9.1 %collective-permute-start = (f32[4,64,64]{2,1,0:T(8,128)S(1)}, f32[4,64,64]{2,1,0:T(8,128)S(1)}, u32[]{:S(2)}, u32[]{:S(2)}) collective-permute-start(f32[4,64,64]{2,1,0:T(8,128)S(1)} %multiply_add_fusion.2), channel_id=1, source_target_pairs={{0,2},{2,4},{4,6},{6,8},{8,10},{10,12},{12,14},{14,16},{16,18},{18... | collective-permute-start | bytes 196616 | tf_op jit(solution)/shard_map/while/body/eval_jaxpr/ppermute | solution.py:19
  117.2 6.3 %collective-permute-start = (f32[4,64,64]{2,1,0:T(8,128)S(1)}, f32[4,64,64]{2,1,0:T(8,128)S(1)}, u32[]{:S(2)}, u32[]{:S(2)}) collective-permute-start(f32[4,64,64]{2,1,0:T(8,128)S(1)} %multiply_add_fusion.2), channel_id=1, source_target_pairs={{0,2},{2,4},{4,6},{6,8},{8,10},{10,12},{12,14},{14,16},{16,18},{18... | collective-permute-start | bytes 196616 | tf_op jit(solution)/shard_map/while/body/eval_jaxpr/ppermute | solution.py:19
  124.6 8.3 %collective-permute-start = (f32[4,64,64]{2,1,0:T(8,128)S(1)}, f32[4,64,64]{2,1,0:T(8,128)S(1)}, u32[]{:S(2)}, u32[]{:S(2)}) collective-permute-start(f32[4,64,64]{2,1,0:T(8,128)S(1)} %multiply_add_fusion.2), channel_id=1, source_target_pairs={{0,2},{2,4},{4,6},{6,8},{8,10},{10,12},{12,14},{14,16},{16,18},{18... | collective-permute-start | bytes 196616 | tf_op jit(solution)/shard_map/while/body/eval_jaxpr/ppermute | solution.py:19
  134.0 7.0 %collective-permute-start = (f32[4,64,64]{2,1,0:T(8,128)S(1)}, f32[4,64,64]{2,1,0:T(8,128)S(1)}, u32[]{:S(2)}, u32[]{:S(2)}) collective-permute-start(f32[4,64,64]{2,1,0:T(8,128)S(1)} %multiply_add_fusion.2), channel_id=1, source_target_pairs={{0,2},{2,4},{4,6},{6,8},{8,10},{10,12},{12,14},{14,16},{16,18},{18... | collective-permute-start | bytes 196616 | tf_op jit(solution)/shard_map/while/body/eval_jaxpr/ppermute | solution.py:19
  142.0 9.2 %collective-permute-start = (f32[4,64,64]{2,1,0:T(8,128)S(1)}, f32[4,64,64]{2,1,0:T(8,128)S(1)}, u32[]{:S(2)}, u32[]{:S(2)}) collective-permute-start(f32[4,64,64]{2,1,0:T(8,128)S(1)} %multiply_add_fusion.2), channel_id=1, source_target_pairs={{0,2},{2,4},{4,6},{6,8},{8,10},{10,12},{12,14},{14,16},{16,18},{18... | collective-permute-start | bytes 196616 | tf_op jit(solution)/shard_map/while/body/eval_jaxpr/ppermute | solution.py:19
  152.3 10.6 %collective-permute-start = (f32[4,64,64]{2,1,0:T(8,128)S(1)}, f32[4,64,64]{2,1,0:T(8,128)S(1)}, u32[]{:S(2)}, u32[]{:S(2)}) collective-permute-start(f32[4,64,64]{2,1,0:T(8,128)S(1)} %multiply_add_fusion.2), channel_id=1, source_target_pairs={{0,2},{2,4},{4,6},{6,8},{8,10},{10,12},{12,14},{14,16},{16,18},{18... | collective-permute-start | bytes 196616 | tf_op jit(solution)/shard_map/while/body/eval_jaxpr/ppermute | solution.py:19
  164.0 8.2 %collective-permute-start = (f32[4,64,64]{2,1,0:T(8,128)S(1)}, f32[4,64,64]{2,1,0:T(8,128)S(1)}, u32[]{:S(2)}, u32[]{:S(2)}) collective-permute-start(f32[4,64,64]{2,1,0:T(8,128)S(1)} %multiply_add_fusion.2), channel_id=1, source_target_pairs={{0,2},{2,4},{4,6},{6,8},{8,10},{10,12},{12,14},{14,16},{16,18},{18... | collective-permute-start | bytes 196616 | tf_op jit(solution)/shard_map/while/body/eval_jaxpr/ppermute | solution.py:19
  173.3 9.1 %collective-permute-start = (f32[4,64,64]{2,1,0:T(8,128)S(1)}, f32[4,64,64]{2,1,0:T(8,128)S(1)}, u32[]{:S(2)}, u32[]{:S(2)}) collective-permute-start(f32[4,64,64]{2,1,0:T(8,128)S(1)} %multiply_add_fusion.2), channel_id=1, source_target_pairs={{0,2},{2,4},{4,6},{6,8},{8,10},{10,12},{12,14},{14,16},{16,18},{18... | collective-permute-start | bytes 196616 | tf_op jit(solution)/shard_map/while/body/eval_jaxpr/ppermute | solution.py:19
  184.2 4.9 %all_gather.15 = bf16[128,512]{0,1:T(8,128)(2,1)S(1)} all-gather(bf16[128,256]{0,1:T(8,128)(2,1)S(1)} %bitcast.118), channel_id=1, replica_groups=mesh['grp'=1,'sp'=16,'tp'=2] {'tp'}, dimensions={1}, use_global_device_ids=true | all-gather | bytes 196608 | tf_op jit(solution)/shard_map/all_gather | solution.py:151
  189.6 4.9 %psum.7 = f32[128]{0:T(128)S(1)} all-reduce(f32[128]{0:T(128)S(1)} %get-tuple-element.142), channel_id=1, replica_groups=mesh['grp'=1,'sp'=16,'tp'=2] {'tp'}, use_global_device_ids=true, to_apply=%region_8.9 | all-reduce | flops 128 | bytes 1024 | tf_op jit(solution)/shard_map/psum | solution.py:156
  194.7 7.1 %all_gather.16 = bf16[128,2048]{1,0:T(8,128)(2,1)S(1)} all-gather(bf16[128,1024]{1,0:T(8,128)(2,1)S(1)} %multiply_convert_fusion), channel_id=1, replica_groups=mesh['grp'=1,'sp'=16,'tp'=2] {'tp'}, dimensions={1}, use_global_device_ids=true | all-gather | bytes 786432 | tf_op jit(solution)/shard_map/all_gather | solution.py:160
  201.7 6.0 %convolution_convert_fusion.1 = bf16[128,2816]{1,0:T(8,128)(2,1)S(1)} fusion(bf16[128,2048]{1,0:T(8,128)(2,1)S(1)} %all_gather.16, bf16[2048,2816]{1,0:T(8,128)(2,1)} %all-gather.4.cloned.1.call-done), kind=kOutput, calls=%fused_computation.28 | convolution fusion | flops 1476755456 | bytes 12779520 | tf_op jit(solution)/shard_map/dot_general | solution.py:161
  207.8 5.0 %all-gather.6.cloned.1.call-done = bf16[2048,2816]{1,0:T(8,128)(2,1)} async-done(((bf16[128,2816]{1,0:T(8,128)(2,1)}), bf16[2048,2816]{1,0:T(8,128)(2,1)}) %all-gather.6.cloned.1.call-update) | async-done | bytes 11534352 | tf_op jit(solution)/shard_map/all_gather | solution.py:168
  212.8 6.0 %convolution_convert_fusion = bf16[128,2816]{1,0:T(8,128)(2,1)S(1)} fusion(bf16[128,2048]{1,0:T(8,128)(2,1)S(1)} %all_gather.16, bf16[2048,2816]{1,0:T(8,128)(2,1)} %all-gather.6.cloned.1.call-done), kind=kOutput, calls=%fused_computation.27 | convolution fusion | flops 1476755456 | bytes 12779520 | tf_op jit(solution)/shard_map/dot_general | solution.py:166
  223.9 88.6 %all-gather.8.cloned.1.call-done = bf16[2816,2048]{1,0:T(8,128)(2,1)} async-done(((bf16[2816,128]{1,0:T(8,128)(2,1)}), bf16[2816,2048]{1,0:T(8,128)(2,1)}) %all-gather.8.cloned.1.call-update) | async-done | bytes 11534352 | tf_op jit(solution)/shard_map/all_gather | solution.py:183
  312.5 10.6 %convolution_convert_fusion.2 = bf16[128,2048]{1,0:T(8,128)(2,1)} fusion(bf16[2816,2048]{1,0:T(8,128)(2,1)} %all-gather.8.cloned.1.call-done, f32[130,2816]{1,0:T(8,128)} %get-tuple-element.145, f32[130,2816]{1,0:T(8,128)} %get-tuple-element.144, f32[2816]{0:T(1024)S(1)} %get-tuple-element.110, f32[2816]{0:T(1024)S(1)} %get-tuple-element.111, ...), kind=kOutput, calls=%fused_computation.29 | convolution fusion | flops 1482424320 | bytes 20776960 | tf_op jit(solution)/shard_map/dot_general | solution.py:181
  323.2 13.0 %reduce-scatter.2.cloned.1.call-done = bf16[128,1024]{1,0:T(8,128)(2,1)} async-done(((bf16[128,2048]{1,0:T(8,128)(2,1)}), bf16[128,1024]{1,0:T(8,128)(2,1)}) %reduce-scatter.2.cloned.1.call-update) | async-done | bytes 262160 | tf_op jit(solution)/shard_map/reduce_scatter | solution.py:186
  (123 shorter events, 34.5 us)
Async XLA Ops:
  6.5 182.6 %copy-start = (bf16[512,1024]{1,0:T(8,128)(2,1)S(1)}, bf16[512,1024]{1,0:T(8,128)(2,1)}, u32[]{:S(2)}) copy-start(bf16[512,1024]{1,0:T(8,128)(2,1)} %param.25) | copy-start | bytes 3145732
  6.5 2.3 copy-start.2
  6.5 2.4 copy-start.9
  6.5 2.9 copy-start.3
  6.5 195.2 %all-gather.4.cloned.1.call-start = ((), (), s32[]{:S(2)}) async-start(), calls=%async_computation.1 | async-start | bytes 12255232 | tf_op jit(solution)/shard_map/all_gather | solution.py:163
  7.3 205.6 %all-gather.6.cloned.1.call-start = ((), (), s32[]{:S(2)}) async-start(), calls=%async_computation.2 | async-start | bytes 12255232 | tf_op jit(solution)/shard_map/all_gather | solution.py:168
  8.0 304.5 %all-gather.8.cloned.1.call-start = ((), (), s32[]{:S(2)}) async-start(), calls=%async_computation.3 | async-start | bytes 12255232 | tf_op jit(solution)/shard_map/all_gather | solution.py:183
  8.8 1.2 copy-start.4
  8.8 327.3 %reduce-scatter.2.cloned.1.call-start = ((), (), s32[]{:S(2)}) async-start(), calls=%async_computation.4 | async-start | bytes 786432 | tf_op jit(solution)/shard_map/reduce_scatter | solution.py:186
  10.6 44.1 %copy-start.5 = (bf16[128,256]{1,0:T(8,128)(2,1)S(1)}, bf16[128,256]{1,0:T(8,128)(2,1)}, u32[]{:S(2)}) copy-start(bf16[128,256]{1,0:T(8,128)(2,1)} %param.22) | copy-start | bytes 196612
  54.9 129.3 %copy-start.10 = (f32[64]{0:T(128)S(1)}, f32[64]{0:T(128)}, u32[]{:S(2)}) copy-start(f32[64]{0:T(128)} %param.24) | copy-start | bytes 772
  54.9 134.3 %copy-start.1 = (bf16[128,1024]{1,0:T(8,128)(2,1)S(1)}, bf16[128,1024]{1,0:T(8,128)(2,1)}, u32[]{:S(2)}) copy-start(bf16[128,1024]{1,0:T(8,128)(2,1)} %param.18) | copy-start | bytes 786436
  55.0 3.4 collective-permute-start
  58.5 9.3 %collective-permute-start = (f32[4,64,64]{2,1,0:T(8,128)S(1)}, f32[4,64,64]{2,1,0:T(8,128)S(1)}, u32[]{:S(2)}, u32[]{:S(2)}) collective-permute-start(f32[4,64,64]{2,1,0:T(8,128)S(1)} %multiply_add_fusion.2), channel_id=1, source_target_pairs={{0,2},{2,4},{4,6},{6,8},{8,10},{10,12},{12,14},{14,16},{16,18},{18... | collective-permute-start | bytes 196616 | tf_op jit(solution)/shard_map/while/body/eval_jaxpr/ppermute | solution.py:19
  67.9 9.2 %collective-permute-start = (f32[4,64,64]{2,1,0:T(8,128)S(1)}, f32[4,64,64]{2,1,0:T(8,128)S(1)}, u32[]{:S(2)}, u32[]{:S(2)}) collective-permute-start(f32[4,64,64]{2,1,0:T(8,128)S(1)} %multiply_add_fusion.2), channel_id=1, source_target_pairs={{0,2},{2,4},{4,6},{6,8},{8,10},{10,12},{12,14},{14,16},{16,18},{18... | collective-permute-start | bytes 196616 | tf_op jit(solution)/shard_map/while/body/eval_jaxpr/ppermute | solution.py:19
  77.2 9.2 %collective-permute-start = (f32[4,64,64]{2,1,0:T(8,128)S(1)}, f32[4,64,64]{2,1,0:T(8,128)S(1)}, u32[]{:S(2)}, u32[]{:S(2)}) collective-permute-start(f32[4,64,64]{2,1,0:T(8,128)S(1)} %multiply_add_fusion.2), channel_id=1, source_target_pairs={{0,2},{2,4},{4,6},{6,8},{8,10},{10,12},{12,14},{14,16},{16,18},{18... | collective-permute-start | bytes 196616 | tf_op jit(solution)/shard_map/while/body/eval_jaxpr/ppermute | solution.py:19
  86.6 6.3 %collective-permute-start = (f32[4,64,64]{2,1,0:T(8,128)S(1)}, f32[4,64,64]{2,1,0:T(8,128)S(1)}, u32[]{:S(2)}, u32[]{:S(2)}) collective-permute-start(f32[4,64,64]{2,1,0:T(8,128)S(1)} %multiply_add_fusion.2), channel_id=1, source_target_pairs={{0,2},{2,4},{4,6},{6,8},{8,10},{10,12},{12,14},{14,16},{16,18},{18... | collective-permute-start | bytes 196616 | tf_op jit(solution)/shard_map/while/body/eval_jaxpr/ppermute | solution.py:19
  93.0 6.3 %collective-permute-start = (f32[4,64,64]{2,1,0:T(8,128)S(1)}, f32[4,64,64]{2,1,0:T(8,128)S(1)}, u32[]{:S(2)}, u32[]{:S(2)}) collective-permute-start(f32[4,64,64]{2,1,0:T(8,128)S(1)} %multiply_add_fusion.2), channel_id=1, source_target_pairs={{0,2},{2,4},{4,6},{6,8},{8,10},{10,12},{12,14},{14,16},{16,18},{18... | collective-permute-start | bytes 196616 | tf_op jit(solution)/shard_map/while/body/eval_jaxpr/ppermute | solution.py:19
  99.4 7.6 %collective-permute-start = (f32[4,64,64]{2,1,0:T(8,128)S(1)}, f32[4,64,64]{2,1,0:T(8,128)S(1)}, u32[]{:S(2)}, u32[]{:S(2)}) collective-permute-start(f32[4,64,64]{2,1,0:T(8,128)S(1)} %multiply_add_fusion.2), channel_id=1, source_target_pairs={{0,2},{2,4},{4,6},{6,8},{8,10},{10,12},{12,14},{14,16},{16,18},{18... | collective-permute-start | bytes 196616 | tf_op jit(solution)/shard_map/while/body/eval_jaxpr/ppermute | solution.py:19
  107.1 10.1 %collective-permute-start = (f32[4,64,64]{2,1,0:T(8,128)S(1)}, f32[4,64,64]{2,1,0:T(8,128)S(1)}, u32[]{:S(2)}, u32[]{:S(2)}) collective-permute-start(f32[4,64,64]{2,1,0:T(8,128)S(1)} %multiply_add_fusion.2), channel_id=1, source_target_pairs={{0,2},{2,4},{4,6},{6,8},{8,10},{10,12},{12,14},{14,16},{16,18},{18... | collective-permute-start | bytes 196616 | tf_op jit(solution)/shard_map/while/body/eval_jaxpr/ppermute | solution.py:19
  117.2 7.2 %collective-permute-start = (f32[4,64,64]{2,1,0:T(8,128)S(1)}, f32[4,64,64]{2,1,0:T(8,128)S(1)}, u32[]{:S(2)}, u32[]{:S(2)}) collective-permute-start(f32[4,64,64]{2,1,0:T(8,128)S(1)} %multiply_add_fusion.2), channel_id=1, source_target_pairs={{0,2},{2,4},{4,6},{6,8},{8,10},{10,12},{12,14},{14,16},{16,18},{18... | collective-permute-start | bytes 196616 | tf_op jit(solution)/shard_map/while/body/eval_jaxpr/ppermute | solution.py:19
  124.6 9.3 %collective-permute-start = (f32[4,64,64]{2,1,0:T(8,128)S(1)}, f32[4,64,64]{2,1,0:T(8,128)S(1)}, u32[]{:S(2)}, u32[]{:S(2)}) collective-permute-start(f32[4,64,64]{2,1,0:T(8,128)S(1)} %multiply_add_fusion.2), channel_id=1, source_target_pairs={{0,2},{2,4},{4,6},{6,8},{8,10},{10,12},{12,14},{14,16},{16,18},{18... | collective-permute-start | bytes 196616 | tf_op jit(solution)/shard_map/while/body/eval_jaxpr/ppermute | solution.py:19
  134.0 8.0 %collective-permute-start = (f32[4,64,64]{2,1,0:T(8,128)S(1)}, f32[4,64,64]{2,1,0:T(8,128)S(1)}, u32[]{:S(2)}, u32[]{:S(2)}) collective-permute-start(f32[4,64,64]{2,1,0:T(8,128)S(1)} %multiply_add_fusion.2), channel_id=1, source_target_pairs={{0,2},{2,4},{4,6},{6,8},{8,10},{10,12},{12,14},{14,16},{16,18},{18... | collective-permute-start | bytes 196616 | tf_op jit(solution)/shard_map/while/body/eval_jaxpr/ppermute | solution.py:19
  142.0 10.1 %collective-permute-start = (f32[4,64,64]{2,1,0:T(8,128)S(1)}, f32[4,64,64]{2,1,0:T(8,128)S(1)}, u32[]{:S(2)}, u32[]{:S(2)}) collective-permute-start(f32[4,64,64]{2,1,0:T(8,128)S(1)} %multiply_add_fusion.2), channel_id=1, source_target_pairs={{0,2},{2,4},{4,6},{6,8},{8,10},{10,12},{12,14},{14,16},{16,18},{18... | collective-permute-start | bytes 196616 | tf_op jit(solution)/shard_map/while/body/eval_jaxpr/ppermute | solution.py:19
  152.3 11.6 %collective-permute-start = (f32[4,64,64]{2,1,0:T(8,128)S(1)}, f32[4,64,64]{2,1,0:T(8,128)S(1)}, u32[]{:S(2)}, u32[]{:S(2)}) collective-permute-start(f32[4,64,64]{2,1,0:T(8,128)S(1)} %multiply_add_fusion.2), channel_id=1, source_target_pairs={{0,2},{2,4},{4,6},{6,8},{8,10},{10,12},{12,14},{14,16},{16,18},{18... | collective-permute-start | bytes 196616 | tf_op jit(solution)/shard_map/while/body/eval_jaxpr/ppermute | solution.py:19
  164.0 9.2 %collective-permute-start = (f32[4,64,64]{2,1,0:T(8,128)S(1)}, f32[4,64,64]{2,1,0:T(8,128)S(1)}, u32[]{:S(2)}, u32[]{:S(2)}) collective-permute-start(f32[4,64,64]{2,1,0:T(8,128)S(1)} %multiply_add_fusion.2), channel_id=1, source_target_pairs={{0,2},{2,4},{4,6},{6,8},{8,10},{10,12},{12,14},{14,16},{16,18},{18... | collective-permute-start | bytes 196616 | tf_op jit(solution)/shard_map/while/body/eval_jaxpr/ppermute | solution.py:19
  173.3 10.1 %collective-permute-start = (f32[4,64,64]{2,1,0:T(8,128)S(1)}, f32[4,64,64]{2,1,0:T(8,128)S(1)}, u32[]{:S(2)}, u32[]{:S(2)}) collective-permute-start(f32[4,64,64]{2,1,0:T(8,128)S(1)} %multiply_add_fusion.2), channel_id=1, source_target_pairs={{0,2},{2,4},{4,6},{6,8},{8,10},{10,12},{12,14},{14,16},{16,18},{18... | collective-permute-start | bytes 196616 | tf_op jit(solution)/shard_map/while/body/eval_jaxpr/ppermute | solution.py:19
  184.1 10.5 %copy-start.8 = (f32[1024]{0:T(1024)S(1)}, f32[1024]{0:T(1024)}, u32[]{:S(2)}) copy-start(f32[1024]{0:T(1024)} %param.26) | copy-start | bytes 12292
  207.8 13.4 %copy-start.6 = (f32[3,2816]{1,0:T(4,128)S(1)}, f32[3,2816]{1,0:T(4,128)}, u32[]{:S(2)}) copy-start(f32[3,2816]{1,0:T(4,128)} %param.29) | copy-start | bytes 101380
  207.8 13.4 %copy-start.7 = (f32[3,2816]{1,0:T(4,128)S(1)}, f32[3,2816]{1,0:T(4,128)}, u32[]{:S(2)}) copy-start(f32[3,2816]{1,0:T(4,128)} %param.30) | copy-start | bytes 101380
  218.8 3.0 collective-permute-start.1
Sparse Core Ops, SparseCore 0:
  9.6 99.5 all-gather.3
  111.5 101.2 all-gather.5
  215.0 97.4 all-gather.7
  323.3 12.7 reduce-scatter.1
where the time goes:
time: 345 us; the launch traced here: 344 us
  waiting for transfers between devices  124 us (36%)
  starting transfers between devices  115 us (33%)
  matrix products  27.1 us (8%)
  other arithmetic  25.4 us (7%)
  local copies, waits for them, and re-layouts  22.6 us (7%)
  blocking collectives  17 us (5%)
  between operations  13.5 us (4%)
    ppermute x16, starting transfers between devices, shifted(): return lax.ppermute(array, axis, pairs)  115 us
    all_gather x1, waiting for transfers between devices, on_device(): lax.all_gather(down_weight, 'sp', axis=1, tiled=True)  88.6 us
    while x2, local copies, waits for them, and re-layouts  18.2 us
    ppermute x16, waiting for transfers between devices, shifted(): return lax.ppermute(array, axis, pairs)  14.8 us
    reduce_scatter x1, waiting for transfers between devices, on_device(): lax.psum_scatter(terms.astype(jnp.bfloat16), 'tp', scatter_dimension=1, t...  13 us
    dot_general x1, matrix products, on_device(): jnp.dot(hidden, lax.all_gather(down_weight, 'sp', axis=1, tiled=True), pr...  10.6 us
    dot_general x2, other arithmetic, advance(): jnp.einsum('htk,hsk,htsk->hts', block_queries, block_keys, jnp.exp(spread...  10.5 us
    exp x2, other arithmetic, advance(): jnp.exp(spread)  8.67 us
  transfers between devices with their start and end apart: 20, of which 19 were waited for; matrix products, arithmetic and copies ran while one was open for 18% of the time, Pallas kernels for 0%

commit v1 on v0

v1 whole, which is shorter than its diff:
```python
import jax
import jax.numpy as jnp
from jax import lax
from jax.sharding import PartitionSpec as P

DK = 64
SUB = 16
epsilon = 1e-06
highest = lax.Precision.HIGHEST
f32 = jnp.float32
bf16 = jnp.bfloat16


def local_recurrence(query_pre, forget_pre, value_pre, floor_gap):
    rows, width = query_pre.shape
    heads = width // DK
    subs = rows // SUB
    keys = floor_gap * jax.nn.sigmoid(-forget_pre.astype(f32))
    log_decay = jnp.log1p(-keys)
    query = jax.nn.silu(query_pre.astype(f32))
    values = value_pre.astype(f32)
    position = lax.iota(jnp.int32, rows)
    lower = (position[:, None] >= position[None, :]).astype(f32)
    running = jnp.dot(lower, log_decay, precision=highest)
    middle = running.reshape(subs, SUB, width)[:, SUB // 2 - 1, :]
    query_part = query * jnp.exp(running - jnp.repeat(middle, SUB, axis=0))
    reach = (lax.iota(jnp.int32, subs) + 1) * SUB
    seen = position[None, :, None] < reach[:, None, None]
    key_part = keys[None] * jnp.exp(
        jnp.where(seen, middle[:, None, :] - running[None], -jnp.inf)
    )
    scores = jnp.einsum(
        "ithk,ishk->hits",
        query_part.reshape(subs, SUB, heads, DK),
        key_part.reshape(subs, rows, heads, DK),
        precision=highest,
    ).reshape(heads, rows, rows)
    scores = jnp.where(position[None, :, None] >= position[None, None, :], scores, 0.0)
    value_heads = values.reshape(rows, heads, DK)
    inner = jnp.einsum("hts,shv->htv", scores, value_heads, precision=highest)
    ending = running[-1]
    state = jnp.einsum(
        "shv,shk->vhk",
        value_heads,
        (keys * jnp.exp(ending - running)).reshape(rows, heads, DK),
        precision=highest,
    ).reshape(DK, width)
    from_start = (query * jnp.exp(running)).reshape(rows, heads, DK)
    return inner, state, jnp.exp(ending), from_start


def causal_taps(before, current, taps):
    padded = jnp.concatenate([before, current], axis=1).astype(f32)
    rows = current.shape[1]
    return (
        taps[0] * padded[:, 0:rows]
        + taps[1] * padded[:, 1 : rows + 1]
        + taps[2] * padded[:, 2 : rows + 2]
    )


def on_device(
    residual_in,
    query_pre,
    forget_pre,
    value_pre,
    gate_pre,
    floor_gap,
    head_gain,
    out_weight,
    norm_gain,
    value_weight,
    gate_weight,
    value_taps,
    gate_taps,
    down_weight,
):
    sp = lax.axis_size("sp")
    tp = lax.axis_size("tp")
    inner_size = 4 if sp % 4 == 0 else 1
    outer = sp // inner_size
    me = lax.axis_index("sp")
    my_outer = me // inner_size
    my_inner = me % inner_size
    outer_groups = [[o * inner_size + i for o in range(outer)] for i in range(inner_size)]
    inner_groups = [[o * inner_size + i for i in range(inner_size)] for o in range(outer)]
    rows, my_width = residual_in.shape
    width = my_width * tp
    depth, half = value_weight.shape
    chunk = half // outer

    def exchange(array):
        return lax.all_to_all(
            array, "sp", 0, 0, axis_index_groups=outer_groups, tiled=True
        )

    def gather_inner(array):
        return lax.all_gather(array, "sp", axis_index_groups=inner_groups)

    up_pair = jnp.stack([value_weight, gate_weight]).reshape(2, depth, outer, chunk)
    up_pair = up_pair.transpose(2, 0, 1, 3)
    down_part = down_weight.reshape(outer, chunk, depth)
    up_mine = gather_inner(exchange(up_pair))
    down_mine = gather_inner(exchange(down_part))
    value_chunk = up_mine[:, :, 0].reshape(width, chunk)
    gate_chunk = up_mine[:, :, 1].reshape(width, chunk)
    down_chunk = down_mine.transpose(2, 1, 0, 3).reshape(chunk, width)

    out_full = lax.all_gather(out_weight, "tp", axis=1, tiled=True)
    gain_full = lax.all_gather(norm_gain, "tp", axis=0, tiled=True)
    residual_rows = lax.all_gather(residual_in, "tp", axis=1, tiled=True)
    residual_group = lax.all_gather(
        residual_rows, "sp", axis=0, tiled=True, axis_index_groups=outer_groups
    )

    inner, state, total_decay, from_start = local_recurrence(
        query_pre, forget_pre, value_pre, floor_gap
    )
    heads = inner.shape[0]
    packed = jnp.concatenate([state, jnp.broadcast_to(total_decay, (8, heads * DK))], axis=0)
    everyone = lax.all_gather(packed, "sp")
    entering = jnp.zeros_like(state)
    for j in range(sp - 1):
        advanced = entering * everyone[j, DK] + everyone[j, :DK]
        entering = jnp.where(j < me, advanced, entering)
    carried = jnp.einsum(
        "thk,vhk->htv", from_start, entering.reshape(DK, heads, DK), precision=highest
    )
    recurrent = (inner + carried).transpose(1, 0, 2)
    scaled = (
        recurrent
        * lax.rsqrt(jnp.mean(recurrent * recurrent, axis=-1, keepdims=True) + epsilon)
        * head_gain
    )
    gating = jax.nn.silu(gate_pre.astype(f32)).reshape(recurrent.shape)
    head_out = (scaled * gating).reshape(rows, heads * DK).astype(bf16)

    head_rows = lax.all_gather(head_out, "tp", axis=1, tiled=True)
    head_group = lax.all_gather(
        head_rows, "sp", axis=0, tiled=True, axis_index_groups=outer_groups
    )
    stream = residual_group.astype(f32) + jnp.dot(
        head_group, out_full, preferred_element_type=f32
    )
    squares = jnp.mean(stream * stream, axis=1, keepdims=True)
    normed = (stream * lax.rsqrt(squares + epsilon) * gain_full).astype(bf16)
    normed = (
        normed.reshape(outer * rows, outer, inner_size, depth)
        .transpose(0, 2, 1, 3)
        .reshape(outer * rows, width)
    )
    up_value = jnp.dot(normed, value_chunk, preferred_element_type=f32).astype(bf16)
    up_gate = jnp.dot(normed, gate_chunk, preferred_element_type=f32).astype(bf16)
    up_value = up_value.reshape(outer, rows, chunk)
    up_gate = up_gate.reshape(outer, rows, chunk)
    tails = jnp.concatenate([up_value[:, rows - 2 :], up_gate[:, rows - 2 :]], axis=2)
    pairs = [
        (o * inner_size + i, o * inner_size + (i + 1) % inner_size)
        for o in range(outer)
        for i in range(inner_size)
    ]
    arrived = lax.ppermute(tails, "sp", pairs) if inner_size > 1 else tails
    wrapped = jnp.concatenate([jnp.zeros_like(arrived[:1]), arrived[:-1]], axis=0)
    before = jnp.where(my_inner == 0, wrapped, arrived)

    my_taps = lambda taps: lax.dynamic_slice_in_dim(taps, my_outer * chunk, chunk, axis=1)
    conv_value = causal_taps(before[:, :, :chunk], up_value, my_taps(value_taps))
    conv_gate = causal_taps(before[:, :, chunk:], up_gate, my_taps(gate_taps))
    hidden = (jax.nn.silu(conv_gate) * conv_value).astype(bf16)
    terms = jnp.dot(
        hidden.reshape(outer * rows, chunk), down_chunk, preferred_element_type=f32
    ).astype(bf16)
    summed = lax.psum_scatter(
        terms, "sp", scatter_dimension=0, tiled=True, axis_index_groups=outer_groups
    )
    summed = lax.psum_scatter(summed, "tp", scatter_dimension=1, tiled=True)
    own = lax.dynamic_slice(
        stream, (my_outer * rows, lax.axis_index("tp") * my_width), (rows, my_width)
    )
    return (own + summed.astype(f32)).astype(bf16)


def solution(mesh):
    rows = P(("grp", "sp"), "tp")
    return jax.shard_map(
        on_device,
        mesh=mesh,
        in_specs=(
            rows,
            rows,
            rows,
            rows,
            rows,
            P("tp"),
            P(),
            P(None, "tp"),
            P("tp"),
            P("sp", "tp"),
            P("sp", "tp"),
            P(None, "tp"),
            P(None, "tp"),
            P("tp", "sp"),
        ),
        out_specs=rows,
        check_vma=False,
    )
```

time: 345 us -> 317 us (0.919)
  starting transfers between devices: 115 us -> 4.29 us
  blocking collectives: 17 us -> 89.5 us
  local copies, waits for them, and re-layouts: 22.6 us -> 48.8 us
  matrix products: 27.1 us -> 18.5 us
  other arithmetic: 25.4 us -> 19.8 us
    ppermute x16 -> x1, starting transfers between devices: 115 us -> 0.41 us  [on_device(): arrived = lax.ppermute(tails, 'sp', pairs) if inner_size > 1 else tails]
    reduce_scatter x1 -> x2, waiting for transfers between devices: 13 us -> 60.9 us  [the longest x1 44.9 us: on_device(): lax.psum_scatter(terms, 'sp', scatter_dimension=0, tiled=True, axis_index...]
    all_gather x3 -> x5, waiting for transfers between devices: 93.7 us -> 49.2 us  [the longest x2 29.5 us: gather_inner(): return lax.all_gather(array, 'sp', axis_index_groups=inner_groups)]
    all_to_all x0 -> x1, blocking collectives: none -> 44 us  [exchange(): lax.all_to_all(array, 'sp', 0, 0, axis_index_groups=outer_groups, tiled=T...]
    all_gather x2 -> x4, blocking collectives: 12 us -> 45.5 us  [the longest x1 25.9 us: on_device(): lax.all_gather(head_rows, 'sp', axis=0, tiled=True, axis_index_groups=out...]
    while x2 -> x0, local copies, waits for them, and re-layouts: 18.2 us -> none
    slice x6 -> x12, local copies, waits for them, and re-layouts: 0.24 us -> 16.8 us  [the longest x2 8.79 us: on_device(): gate_chunk = up_mine[:, :, 1].reshape(width, chunk)]
    ppermute x16 -> x1, waiting for transfers between devices: 14.8 us -> 0.01 us  [on_device(): arrived = lax.ppermute(tails, 'sp', pairs) if inner_size > 1 else tails]
  transfers between devices with their start and end apart: 20 -> 9, of which waited for: 19 -> 5; matrix products, arithmetic and copies ran while one was open for 18% -> 18% of each run, Pallas kernels for 0% -> 0%
where the time goes in v1:
time: 317 us; the launch traced here: 316 us
  waiting for transfers between devices  122 us (38%)
  blocking collectives  89.5 us (28%)
  local copies, waits for them, and re-layouts  48.8 us (15%)
  other arithmetic  19.8 us (6%)
  matrix products  18.5 us (6%)
  between operations  14 us (4%)
  starting transfers between devices  4.29 us (1%)
    reduce_scatter x1, waiting for transfers between devices, on_device(): lax.psum_scatter(terms, 'sp', scatter_dimension=0, tiled=True, axis_index...  44.9 us
    all_to_all x1, blocking collectives, exchange(): lax.all_to_all(array, 'sp', 0, 0, axis_index_groups=outer_groups, tiled=T...  44 us
    all_gather x2, waiting for transfers between devices, gather_inner(): return lax.all_gather(array, 'sp', axis_index_groups=inner_groups)  29.5 us
    all_gather x1, blocking collectives, on_device(): lax.all_gather(head_rows, 'sp', axis=0, tiled=True, axis_index_groups=out...  25.9 us
    all_gather x1, waiting for transfers between devices, on_device(): lax.all_gather(residual_rows, 'sp', axis=0, tiled=True, axis_index_groups...  19.7 us
    reduce_scatter x1, waiting for transfers between devices, on_device(): summed = lax.psum_scatter(summed, 'tp', scatter_dimension=1, tiled=True)  16.1 us
    all_to_all x1, waiting for transfers between devices, exchange(): lax.all_to_all(array, 'sp', 0, 0, axis_index_groups=outer_groups, tiled=T...  10.8 us
    all_gather x1, blocking collectives, on_device(): residual_rows = lax.all_gather(residual_in, 'tp', axis=1, tiled=True)  10 us
  transfers between devices with their start and end apart: 9, of which 5 were waited for; matrix products, arithmetic and copies ran while one was open for 18% of the time, Pallas kernels for 0%

profile of v1, /device:TPU:0, one launch (start us, length us, event | category | flops | bytes accessed | tf_op | source)
XLA Modules:
  0.0 316.4 jit_solution(16694360619134065643)
XLA Ops:
  11.8 10.0 %all_gather.36 = bf16[128,2048]{1,0:T(8,128)(2,1)} all-gather(bf16[128,1024]{1,0:T(8,128)(2,1)S(1)} %copy-done.7), channel_id=1, replica_groups=mesh['grp'=1,'sp'=16,'tp'=2] {'tp'}, dimensions={1}, use_global_device_ids=true | all-gather | bytes 786432 | tf_op jit(solution)/shard_map/all_gather | solution.py:111
  22.8 44.0 %all_to_all.10 = bf16[4,2,128,704]{2,3,1,0:T(8,128)(2,1)} all-to-all(bf16[4,2,128,704]{2,3,1,0:T(8,128)(2,1)S(1)} %copy.91), channel_id=1, replica_groups={{0,8,16,24},{2,10,18,26},{4,12,20,28},{6,14,22,30},{1,9,17,25},{3,11,19..., dimensions={0} | all-to-all | bytes 2883584 | tf_op jit(solution)/shard_map/all_to_all | solution.py:93
  66.9 3.6 %all-to-all-start.1 = ((bf16[4,704,128]{2,1,0:T(8,128)(2,1)}), bf16[4,704,128]{2,1,0:T(8,128)(2,1)S(1)}, u32[]{:S(2)}, u32[]{:S(2)}) async-start(bf16[4,704,128]{2,1,0:T(8,128)(2,1)} %bitcast.22), calls=%async_computation.1 | async-start | bytes 1441792 | tf_op jit(solution)/shard_map/all_to_all | solution.py:93
  71.3 4.6 %all_gather.43 = f32[2048]{0:T(1024)S(1)} all-gather(f32[1024]{0:T(1024)S(1)} %copy-done.9), channel_id=1, replica_groups=mesh['grp'=1,'sp'=16,'tp'=2] {'tp'}, dimensions={0}, use_global_device_ids=true | all-gather | bytes 12288 | tf_op jit(solution)/shard_map/all_gather | solution.py:110
  77.6 10.8 %all-to-all-done.1 = bf16[4,704,128]{2,1,0:T(8,128)(2,1)S(1)} async-done(((bf16[4,704,128]{2,1,0:T(8,128)(2,1)}), bf16[4,704,128]{2,1,0:T(8,128)(2,1)S(1)}, u32[]{:S(2)}, u32[]{:S(2)}) %all-to-all-start.1) | async-done | bytes 720928 | tf_op jit(solution)/shard_map/all_to_all | solution.py:93
  89.4 1.3 fusion.35
  95.4 4.9 %all_gather.40 = bf16[128,512]{0,1:T(8,128)(2,1)S(1)} all-gather(bf16[128,256]{0,1:T(8,128)(2,1)S(1)} %bitcast.81), channel_id=1, replica_groups=mesh['grp'=1,'sp'=16,'tp'=2] {'tp'}, dimensions={1}, use_global_device_ids=true | all-gather | bytes 196608 | tf_op jit(solution)/shard_map/all_gather | solution.py:138
  100.3 25.9 %all_gather.41 = bf16[512,512]{0,1:T(8,128)(2,1)S(1)} all-gather(bf16[128,512]{0,1:T(8,128)(2,1)S(1)} %all_gather.40), channel_id=1, replica_groups={{0,8,16,24},{2,10,18,26},{4,12,20,28},{6,14,22,30},{1,9,17,25},{3,11,19..., dimensions={0}, use_global_device_ids=true | all-gather | bytes 655360 | tf_op jit(solution)/shard_map/all_gather | solution.py:139
  126.3 19.7 %all-gather.9.cloned.1.call-done = bf16[512,2048]{1,0:T(8,128)(2,1)} async-done(((bf16[128,2048]{1,0:T(8,128)(2,1)}), bf16[512,2048]{1,0:T(8,128)(2,1)}) %all-gather.9.cloned.1.call-update) | async-done | bytes 2097168 | tf_op jit(solution)/shard_map/all_gather | solution.py:112
  146.0 3.7 %multiply_reduce_fusion = (f32[512]{0:T(512)S(1)}, f32[512,2048]{1,0:T(8,128)S(1)}) fusion(bf16[512,512]{0,1:T(8,128)(2,1)S(1)} %all_gather.41, bf16[512,2048]{1,0:T(8,128)(2,1)} %all-gather.11.cloned.1.call-done, bf16[512,2048]{1,0:T(8,128)(2,1)} %all-gather.9.cloned.1.call-done), kind=kOutput, calls=%fused_computation.1 | convolution fusion | flops 1077935616 | bytes 8914944 | tf_op jit(solution)/shard_map/dot_general | solution.py:142
  149.7 2.0 copy-done
  152.1 2.9 reshape.247
  155.0 4.3 %copy.88 = bf16[512,4,4,128]{0,3,1,2:T(8,128)(2,1)} copy(bf16[512,4,4,128]{3,2,1,0:T(4,128)(2,1)} %reshape.247) | data formatting | bytes 4194304 | tf_op jit(solution)/shard_map/reshape | solution.py:148
  159.4 29.4 %all-gather.15.cloned.1.call-done = bf16[16,2,128,704]{2,3,1,0:T(8,128)(2,1)} async-done(((bf16[4,2,128,704]{2,3,1,0:T(8,128)(2,1)}), bf16[16,2,128,704]{2,3,1,0:T(8,128)(2,1)}) %all-gather.15.cloned.1.call-update) | async-done | bytes 5767184 | tf_op jit(solution)/shard_map/all_gather | solution.py:98
  188.8 4.7 %fusion.34 = (bf16[4,4,1,128,704]{3,4,2,1,0:T(8,128)(2,1)}, bf16[4,4,1,128,704]{3,4,2,1,0:T(8,128)(2,1)S(1)}) fusion(bf16[4,4,2,128,704]{3,4,2,1,0:T(8,128)(2,1)} %bitcast.65), kind=kLoop, calls=%fused_computation.95 | loop fusion | bytes 11534336 | tf_op jit(solution)/shard_map/slice | solution.py:106
  193.5 2.2 copy.92
  195.7 3.4 %reshape_squeeze.6 = bf16[2048,704]{0,1:T(8,128)(2,1)} reshape(bf16[4,4,1,128,704]{3,1,0,4,2:T(4,128)(2,1)S(1)} %copy.92) | data formatting | bytes 5767168 | tf_op jit(solution)/shard_map/reshape;squeeze | solution.py:105
  199.1 4.1 %convolution_convert_fusion.2 = bf16[512,704]{0,1:T(8,128)(2,1)S(1)} fusion(bf16[2048,704]{0,1:T(8,128)(2,1)} %reshape_squeeze.6, bf16[512,2048]{0,1:T(8,128)(2,1)} %bitcast.69), kind=kOutput, calls=%fused_computation.21 | convolution fusion | flops 1476755456 | bytes 5701632 | tf_op jit(solution)/shard_map/dot_general | solution.py:152
  204.3 4.1 %copy.94 = bf16[4,4,1,128,704]{3,1,0,4,2:T(4,128)(2,1)S(1)} copy(bf16[4,4,1,128,704]{3,4,2,1,0:T(8,128)(2,1)} %get-tuple-element.26) | data formatting | bytes 5767168 | tf_op jit(solution)/shard_map/slice | solution.py:106
  208.4 3.4 %reshape_squeeze.7 = bf16[2048,704]{0,1:T(8,128)(2,1)} reshape(bf16[4,4,1,128,704]{3,1,0,4,2:T(4,128)(2,1)S(1)} %copy.94) | data formatting | bytes 5767168 | tf_op jit(solution)/shard_map/reshape;squeeze | solution.py:106
  211.7 4.1 %convolution_convert_fusion.1 = bf16[512,704]{0,1:T(8,128)(2,1)S(1)} fusion(bf16[2048,704]{0,1:T(8,128)(2,1)} %reshape_squeeze.7, bf16[512,2048]{0,1:T(8,128)(2,1)} %bitcast.70), kind=kOutput, calls=%fused_computation.20 | convolution fusion | flops 1476755456 | bytes 5701632 | tf_op jit(solution)/shard_map/dot_general | solution.py:153
  219.4 4.0 %copy.98 = bf16[704,4,4,128]{3,2,1,0:T(4,128)(2,1)S(1)} copy(bf16[704,4,4,128]{3,0,1,2:T(8,128)(2,1)} %bitcast.66) | data formatting | bytes 5767168 | tf_op jit(solution)/shard_map/transpose | solution.py:107
  223.5 3.4 %reshape.253 = bf16[704,2048]{1,0:T(8,128)(2,1)} reshape(bf16[704,4,4,128]{3,2,1,0:T(4,128)(2,1)S(1)} %copy.98) | data formatting | bytes 5767168 | tf_op jit(solution)/shard_map/reshape | solution.py:107
  227.0 1.3 copy.97
  228.2 2.6 maximum_convert_fusion.1
  230.8 1.3 copy.96
  232.0 2.6 maximum_convert_fusion
  234.6 8.8 %fusion.5 = bf16[4,128,704]{1,0,2:T(4,128)(2,1)S(1)} fusion(f32[4,130,704]{1,0,2:T(4,128)S(1)} %maximum_convert_fusion.1, f32[4,130,704]{1,0,2:T(4,128)S(1)} %maximum_convert_fusion, f32[704]{0:T(1024)S(1)} %get-tuple-element.25, f32[704]{0:T(1024)S(1)} %get-tuple-element.24, f32[704]{0:T(1024)S(1)} %get-tuple-element.23, f32[704]{0:T(1024)S(1)} %get-tuple-element.55, ...), kind=kLoop, calls=%fused_computation.19 | loop fusion | flops 5767168 | bytes 9388544 | tf_op jit(solution)/shard_map/convert_element_type | solution.py:169
  243.4 3.2 %convolution_convert_fusion = bf16[512,2048]{1,0:T(8,128)(2,1)} fusion(bf16[704,2048]{1,0:T(8,128)(2,1)S(1)} %copy-done.3, bf16[88,8,4,128]{3,2,1,0:T(4,128)(2,1)S(1)} %bitcast.73), kind=kOutput, calls=%fused_computation.3 | convolution fusion | flops 1477443584 | bytes 5701632 | tf_op jit(solution)/shard_map/dot_general | solution.py:170
  246.7 44.9 %reduce-scatter.3.cloned.1.call-done = bf16[128,2048]{1,0:T(8,128)(2,1)} async-done(((bf16[512,2048]{1,0:T(8,128)(2,1)}), bf16[128,2048]{1,0:T(8,128)(2,1)}) %reduce-scatter.3.cloned.1.call-update) | async-done | bytes 524304 | tf_op jit(solution)/shard_map/reduce_scatter | solution.py:173
  291.6 16.1 %reduce-scatter.5.cloned.1.call-done = bf16[128,1024]{1,0:T(8,128)(2,1)} async-done(((bf16[128,2048]{1,0:T(8,128)(2,1)}), bf16[128,1024]{1,0:T(8,128)(2,1)}) %reduce-scatter.5.cloned.1.call-update) | async-done | bytes 262160 | tf_op jit(solution)/shard_map/reduce_scatter | solution.py:176
  307.7 1.9 add_convert_fusion
  (117 shorter events, 19.2 us)
Async XLA Ops:
  6.5 5.2 %copy-start.7 = (bf16[128,1024]{1,0:T(8,128)(2,1)S(1)}, bf16[128,1024]{1,0:T(8,128)(2,1)}, u32[]{:S(2)}) copy-start(bf16[128,1024]{1,0:T(8,128)(2,1)} %param.14) | copy-start | bytes 786436
  6.5 82.8 %all-gather.13.cloned.1.call-start = ((), (), s32[]{:S(2)}) async-start(), calls=%async_computation.8 | async-start | bytes 1253376 | tf_op jit(solution)/shard_map/all_gather | solution.py:121
  8.7 13.1 %copy-start.5 = (bf16[128,2816]{1,0:T(8,128)(2,1)S(1)}, bf16[128,2816]{1,0:T(8,128)(2,1)}, u32[]{:S(2)}) copy-start(bf16[128,2816]{1,0:T(8,128)(2,1)} %param.24) | copy-start | bytes 2162692
  10.2 12.0 %copy-start.6 = (bf16[128,2816]{1,0:T(8,128)(2,1)S(1)}, bf16[128,2816]{1,0:T(8,128)(2,1)}, u32[]{:S(2)}) copy-start(bf16[128,2816]{1,0:T(8,128)(2,1)} %param.23) | copy-start | bytes 2162692
  11.0 115.3 %all-gather.11.cloned.1.call-start = ((), (), s32[]{:S(2)}) async-start(), calls=%async_computation.5 | async-start | bytes 3145728 | tf_op jit(solution)/shard_map/all_gather | solution.py:109
  11.7 134.3 %all-gather.9.cloned.1.call-start = ((), (), s32[]{:S(2)}) async-start(), calls=%async_computation.4 | async-start | bytes 2621440 | tf_op jit(solution)/shard_map/all_gather | solution.py:112
  21.8 167.0 %all-gather.15.cloned.1.call-start = ((), (), s32[]{:S(2)}) async-start(), calls=%async_computation.9 | async-start | bytes 7208960 | tf_op jit(solution)/shard_map/all_gather | solution.py:98
  66.8 3.7 %copy-start.8 = (bf16[128,256]{1,0:T(8,128)(2,1)S(1)}, bf16[128,256]{1,0:T(8,128)(2,1)}, u32[]{:S(2)}) copy-start(bf16[128,256]{1,0:T(8,128)(2,1)} %param.18) | copy-start | bytes 196612
  66.8 4.5 %copy-start.9 = (f32[1024]{0:T(1024)S(1)}, f32[1024]{0:T(1024)}, u32[]{:S(2)}) copy-start(f32[1024]{0:T(1024)} %param.22) | copy-start | bytes 12292
  66.9 21.5 %all-to-all-start.1 = ((bf16[4,704,128]{2,1,0:T(8,128)(2,1)}), bf16[4,704,128]{2,1,0:T(8,128)(2,1)S(1)}, u32[]{:S(2)}, u32[]{:S(2)}) async-start(bf16[4,704,128]{2,1,0:T(8,128)(2,1)} %bitcast.22), calls=%async_computation.1 | async-start | bytes 1441792 | tf_op jit(solution)/shard_map/all_to_all | solution.py:93
  70.5 148.9 %all-gather.17.cloned.1.call-start = ((), (), s32[]{:S(2)}) async-start(), calls=%async_computation.10 | async-start | bytes 3604480 | tf_op jit(solution)/shard_map/all_gather | solution.py:98
  88.4 0.9 copy-start.4
  89.3 202.3 %reduce-scatter.3.cloned.1.call-start = ((), (), s32[]{:S(2)}) async-start(), calls=%async_computation.6 | async-start | bytes 2621440 | tf_op jit(solution)/shard_map/reduce_scatter | solution.py:173
  91.6 3.7 %copy-start.10 = (f32[64]{0:T(128)S(1)}, f32[64]{0:T(128)}, u32[]{:S(2)}) copy-start(f32[64]{0:T(128)} %param.20) | copy-start | bytes 772
  149.7 2.0 copy-start
  215.9 1.2 copy-start.1
  216.1 1.9 copy-start.2
  218.0 8.8 %collective-permute-start = (bf16[4,2,1408]{2,0,1:T(4,128)(2,1)S(1)}, bf16[4,2,1408]{2,0,1:T(4,128)(2,1)S(1)}, u32[]{:S(2)}, u32[]{:S(2)}) collective-permute-start(bf16[4,2,1408]{2,0,1:T(4,128)(2,1)S(1)} %pad_maximum_fusion.1), channel_id=1, source_target_pairs={{0,2},{2,4},{4,6},{6,0},{8,10},{10,12},{12,14},{14,8},{16,18},{18,... | collective-permute-start | bytes 67592 | tf_op jit(solution)/shard_map/ppermute | solution.py:162
  234.6 8.8 %copy-start.3 = (bf16[704,2048]{1,0:T(8,128)(2,1)S(1)}, bf16[704,2048]{1,0:T(8,128)(2,1)}, u32[]{:S(2)}) copy-start(bf16[704,2048]{1,0:T(8,128)(2,1)} %reshape.253) | copy-start | bytes 8650756
  246.7 61.0 %reduce-scatter.5.cloned.1.call-start = ((), (), s32[]{:S(2)}) async-start(), calls=%async_computation.7 | async-start | bytes 786432 | tf_op jit(solution)/shard_map/reduce_scatter | solution.py:176
Sparse Core Ops, SparseCore 0:
  11.1 44.8 all-gather.12
  57.5 32.4 all-gather.10
  91.5 54.3 all-gather.8
  147.4 41.3 all-gather.14
  190.2 27.0 all-gather.16
  246.8 44.7 reduce-scatter.2
  293.8 13.8 reduce-scatter.4

commit v2 on v1

--- a/solution.py
+++ b/solution.py
@@ -89,6 +89,10 @@
     depth, half = value_weight.shape
     chunk = half // outer
 
+    wide_groups = [
+        [s * tp + t for s in group for t in range(tp)] for group in outer_groups
+    ]
+
     def exchange(array):
         return lax.all_to_all(
             array, "sp", 0, 0, axis_index_groups=outer_groups, tiled=True
@@ -97,31 +101,59 @@
     def gather_inner(array):
         return lax.all_gather(array, "sp", axis_index_groups=inner_groups)
 
-    up_pair = jnp.stack([value_weight, gate_weight]).reshape(2, depth, outer, chunk)
-    up_pair = up_pair.transpose(2, 0, 1, 3)
-    down_part = down_weight.reshape(outer, chunk, depth)
-    up_mine = gather_inner(exchange(up_pair))
-    down_mine = gather_inner(exchange(down_part))
-    value_chunk = up_mine[:, :, 0].reshape(width, chunk)
-    gate_chunk = up_mine[:, :, 1].reshape(width, chunk)
+    def gather_wide(array):
+        gathered = lax.all_gather(array, ("sp", "tp"), axis_index_groups=wide_groups)
+        gathered = gathered.reshape(outer, tp, *array.shape)
+        return [gathered[:, t].reshape(-1, array.shape[1]) for t in range(tp)]
+
+    def reorder(pieces):
+        span = pieces[0].shape[-1]
+        blocks = []
+        for i in range(inner_size):
+            for o in range(outer):
+                start = (o * inner_size + i) * depth
+                low = start % span
+                blocks.append(pieces[start // span][..., low : low + depth])
+        return lax.optimization_barrier(jnp.concatenate(blocks, axis=-1))
+
+    up_parts = jnp.stack(
+        [
+            jnp.concatenate(
+                [
+                    value_weight[:, o * chunk : (o + 1) * chunk],
+                    gate_weight[:, o * chunk : (o + 1) * chunk],
+                ],
+                axis=1,
+            )
+            for o in range(outer)
+        ]
+    )
+    up_chunk = gather_inner(exchange(up_parts)).reshape(width, 2 * chunk)
+    down_parts = down_weight.reshape(outer, chunk, depth)
+    down_mine = gather_inner(exchange(down_parts))
     down_chunk = down_mine.transpose(2, 1, 0, 3).reshape(chunk, width)
 
-    out_full = lax.all_gather(out_weight, "tp", axis=1, tiled=True)
-    gain_full = lax.all_gather(norm_gain, "tp", axis=0, tiled=True)
-    residual_rows = lax.all_gather(residual_in, "tp", axis=1, tiled=True)
-    residual_group = lax.all_gather(
-        residual_rows, "sp", axis=0, tiled=True, axis_index_groups=outer_groups
-    )
+    out_full = reorder(list(lax.all_gather(out_weight, "tp")))
+    gain_full = reorder(list(lax.all_gather(norm_gain, "tp")))
+    residual_group = reorder(gather_wide(residual_in))
 
     inner, state, total_decay, from_start = local_recurrence(
         query_pre, forget_pre, value_pre, floor_gap
     )
     heads = inner.shape[0]
-    packed = jnp.concatenate([state, jnp.broadcast_to(total_decay, (8, heads * DK))], axis=0)
-    everyone = lax.all_gather(packed, "sp")
+    first = total_decay.astype(bf16)
+    rest = total_decay - first.astype(f32)
+    second = rest.astype(bf16)
+    third = (rest - second.astype(f32)).astype(bf16)
+    spare = jnp.zeros((13, heads * DK), bf16)
+    packed = jnp.concatenate(
+        [state.astype(bf16), first[None], second[None], third[None], spare], axis=0
+    )
+    everyone = lax.all_gather(packed, "sp").astype(f32)
+    decays = everyone[:, DK] + everyone[:, DK + 1] + everyone[:, DK + 2]
     entering = jnp.zeros_like(state)
     for j in range(sp - 1):
-        advanced = entering * everyone[j, DK] + everyone[j, :DK]
+        advanced = entering * decays[j] + everyone[j, :DK]
         entering = jnp.where(j < me, advanced, entering)
     carried = jnp.einsum(
         "thk,vhk->htv", from_start, entering.reshape(DK, heads, DK), precision=highest
@@ -135,25 +167,15 @@
     gating = jax.nn.silu(gate_pre.astype(f32)).reshape(recurrent.shape)
     head_out = (scaled * gating).reshape(rows, heads * DK).astype(bf16)
 
-    head_rows = lax.all_gather(head_out, "tp", axis=1, tiled=True)
-    head_group = lax.all_gather(
-        head_rows, "sp", axis=0, tiled=True, axis_index_groups=outer_groups
-    )
+    head_group = jnp.concatenate(gather_wide(head_out), axis=1)
     stream = residual_group.astype(f32) + jnp.dot(
         head_group, out_full, preferred_element_type=f32
     )
     squares = jnp.mean(stream * stream, axis=1, keepdims=True)
     normed = (stream * lax.rsqrt(squares + epsilon) * gain_full).astype(bf16)
-    normed = (
-        normed.reshape(outer * rows, outer, inner_size, depth)
-        .transpose(0, 2, 1, 3)
-        .reshape(outer * rows, width)
-    )
-    up_value = jnp.dot(normed, value_chunk, preferred_element_type=f32).astype(bf16)
-    up_gate = jnp.dot(normed, gate_chunk, preferred_element_type=f32).astype(bf16)
-    up_value = up_value.reshape(outer, rows, chunk)
-    up_gate = up_gate.reshape(outer, rows, chunk)
-    tails = jnp.concatenate([up_value[:, rows - 2 :], up_gate[:, rows - 2 :]], axis=2)
+    up = jnp.dot(normed, up_chunk, preferred_element_type=f32).astype(bf16)
+    up = up.reshape(outer, rows, 2 * chunk)
+    tails = up[:, rows - 2 :]
     pairs = [
         (o * inner_size + i, o * inner_size + (i + 1) % inner_size)
         for o in range(outer)
@@ -163,19 +185,34 @@
     wrapped = jnp.concatenate([jnp.zeros_like(arrived[:1]), arrived[:-1]], axis=0)
     before = jnp.where(my_inner == 0, wrapped, arrived)
 
-    my_taps = lambda taps: lax.dynamic_slice_in_dim(taps, my_outer * chunk, chunk, axis=1)
-    conv_value = causal_taps(before[:, :, :chunk], up_value, my_taps(value_taps))
-    conv_gate = causal_taps(before[:, :, chunk:], up_gate, my_taps(gate_taps))
-    hidden = (jax.nn.silu(conv_gate) * conv_value).astype(bf16)
+    taps = jnp.concatenate(
+        [
+            lax.dynamic_slice_in_dim(value_taps, my_outer * chunk, chunk, axis=1),
+            lax.dynamic_slice_in_dim(gate_taps, my_outer * chunk, chunk, axis=1),
+        ],
+        axis=1,
+    )
+    conv = causal_taps(before, up, taps)
+    hidden = (jax.nn.silu(conv[:, :, chunk:]) * conv[:, :, :chunk]).astype(bf16)
     terms = jnp.dot(
         hidden.reshape(outer * rows, chunk), down_chunk, preferred_element_type=f32
     ).astype(bf16)
+    terms = jnp.stack(
+        [
+            terms[:, t * my_width : (t + 1) * my_width].reshape(outer, rows, my_width)
+            for t in range(tp)
+        ],
+        axis=1,
+    )
     summed = lax.psum_scatter(
-        terms, "sp", scatter_dimension=0, tiled=True, axis_index_groups=outer_groups
-    )
-    summed = lax.psum_scatter(summed, "tp", scatter_dimension=1, tiled=True)
-    own = lax.dynamic_slice(
-        stream, (my_outer * rows, lax.axis_index("tp") * my_width), (rows, my_width)
+        terms.reshape(outer * tp, rows, my_width),
+        ("sp", "tp"),
+        scatter_dimension=0,
+        axis_index_groups=wide_groups,
+    )
+    my_heads = lax.dynamic_slice_in_dim(head_group, my_outer * rows, rows, axis=0)
+    own = residual_in.astype(f32) + jnp.dot(
+        my_heads, out_weight, preferred_element_type=f32
     )
     return (own + summed.astype(f32)).astype(bf16)
 

time: 317 us -> 275 us (0.87)
  waiting for transfers between devices: 122 us -> 71.8 us
  blocking collectives: 89.5 us -> 113 us
  other arithmetic: 19.8 us -> 8.05 us
  local copies, waits for them, and re-layouts: 48.8 us -> 45.2 us
    all_gather x2, waiting for transfers between devices: 29.5 us -> 0.02 us  [gather_inner(): return lax.all_gather(array, 'sp', axis_index_groups=inner_groups)]
    all_gather x4 -> x3, blocking collectives: 45.5 us -> 72.6 us  [the longest x1 35.8 us: on_device(): everyone = lax.all_gather(packed, 'sp').astype(f32)]
    all_gather x3 -> x2, waiting for transfers between devices: 19.7 us -> 0.04 us  [the longest x1 0.02 us: gather_wide(): lax.all_gather(array, ('sp', 'tp'), axis_index_groups=wide_groups)]
    slice x11 -> x8, local copies, waits for them, and re-layouts: 16.8 us -> 3.68 us  [the longest x2 1.75 us: gather_wide(): return [gathered[:, t].reshape(-1, array.shape[1]) for t in range(tp)]]
    unnamed x28 -> x73, local copies, waits for them, and re-layouts: 5.53 us -> 18.4 us
    all_to_all x1, waiting for transfers between devices: 10.8 us -> 0.01 us  [exchange(): lax.all_to_all(array, 'sp', 0, 0, axis_index_groups=outer_groups, tiled=T...]
    convert_element_type x3, other arithmetic: 11.1 us -> 0.65 us  [the longest x1 0.51 us: on_device(): hidden = (jax.nn.silu(conv[:, :, chunk:]) * conv[:, :, :chunk]).astype(bf16)]
    reduce_scatter x2 -> x1, waiting for transfers between devices: 60.9 us -> 70.3 us  [on_device(): lax.psum_scatter(terms.reshape(outer * tp, rows, my_width), ('sp', 'tp'),...]
  transfers between devices with their start and end apart: 9 -> 7, of which waited for: 5 -> 1; matrix products, arithmetic and copies ran while one was open for 18% -> 22% of each run, Pallas kernels for 0% -> 0%
where the time goes in v2:
time: 275 us; the launch traced here: 274 us
  blocking collectives  113 us (41%)
  waiting for transfers between devices  71.8 us (26%)
  local copies, waits for them, and re-layouts  45.2 us (16%)
  matrix products  17.9 us (7%)
  between operations  14.1 us (5%)
  other arithmetic  8.05 us (3%)
  starting transfers between devices  4.04 us (1%)
    reduce_scatter x1, waiting for transfers between devices, on_device(): lax.psum_scatter(terms.reshape(outer * tp, rows, my_width), ('sp', 'tp'),...  70.3 us
    all_to_all x1, blocking collectives, exchange(): lax.all_to_all(array, 'sp', 0, 0, axis_index_groups=outer_groups, tiled=T...  40.4 us
    all_gather x1, blocking collectives, on_device(): everyone = lax.all_gather(packed, 'sp').astype(f32)  35.8 us
    all_gather x1, blocking collectives, gather_wide(): lax.all_gather(array, ('sp', 'tp'), axis_index_groups=wide_groups)  32.4 us
    unnamed x73, local copies, waits for them, and re-layouts  18.4 us
    mul x14, local copies, waits for them, and re-layouts, on_device(): advanced = entering * decays[j] + everyone[j, :DK]  9.1 us
    dot_general x1, matrix products, on_device(): up = jnp.dot(normed, up_chunk, preferred_element_type=f32).astype(bf16)  7.39 us
  transfers between devices with their start and end apart: 7, of which 1 were waited for; matrix products, arithmetic and copies ran while one was open for 22% of the time, Pallas kernels for 0%

profile of v2, /device:TPU:0, one launch (start us, length us, event | category | flops | bytes accessed | tf_op | source)
XLA Modules:
  0.0 274.1 jit_solution(16133097856761633859)
XLA Ops:
  8.1 1.4 fusion.42
  10.4 40.4 %all_to_all.10 = bf16[4,128,1408]{2,1,0:T(8,128)(2,1)} all-to-all(bf16[4,128,1408]{2,1,0:T(8,128)(2,1)S(1)} %pad_maximum_fusion.1), channel_id=1, replica_groups={{0,8,16,24},{2,10,18,26},{4,12,20,28},{6,14,22,30},{1,9,17,25},{3,11,19..., dimensions={0} | all-to-all | bytes 2883584 | tf_op jit(solution)/shard_map/all_to_all | solution.py:97
  50.8 3.6 %all-to-all-start.1 = ((bf16[4,704,128]{2,1,0:T(8,128)(2,1)}), bf16[4,704,128]{2,1,0:T(8,128)(2,1)S(1)}, u32[]{:S(2)}, u32[]{:S(2)}) async-start(bf16[4,704,128]{2,1,0:T(8,128)(2,1)} %bitcast.45), calls=%async_computation.1 | async-start | bytes 1441792 | tf_op jit(solution)/shard_map/all_to_all | solution.py:97
  56.6 35.8 %all-gather = bf16[1280,256]{1,0:T(8,128)(2,1)S(1)} all-gather(bf16[80,256]{1,0:T(8,128)(2,1)S(1)} %concatenate.36), channel_id=2, replica_groups=mesh['grp'=1,'sp'=16,'tp'=2] {'sp'}, dimensions={0}, use_global_device_ids=true | all-gather | bytes 696320 | tf_op jit(solution)/shard_map/all_gather | solution.py:152
  106.5 2.2 fusion.8
  109.1 1.2 add_select_fusion
  110.8 4.4 %all-gather.3 = f32[2048]{0:T(1024)S(1)} all-gather(f32[1024]{0:T(1024)S(1)} %copy-done.9), channel_id=5, replica_groups=mesh['grp'=1,'sp'=16,'tp'=2] {'tp'}, dimensions={0}, use_global_device_ids=true | all-gather | bytes 12288 | tf_op jit(solution)/shard_map/all_gather | solution.py:137
  115.4 32.4 %all_gather.42 = bf16[8,128,256]{2,1,0:T(8,128)(2,1)S(1)} all-gather(bf16[1,128,256]{2,1,0:T(8,128)(2,1)S(1)} %copy.71), channel_id=1, replica_groups={{0,1,8,9,16,17,24,25},{2,3,10,11,18,19,26,27},{4,5,12,13,20,21,28,29},{..., dimensions={0}, use_global_device_ids=true | all-gather | bytes 589824 | tf_op jit(solution)/shard_map/all_gather | solution.py:105
  150.9 0.9 slice_dynamic-update-slice_fusion.13
  151.8 0.9 slice_dynamic-update-slice_fusion.12
  152.8 0.9 slice_dynamic-update-slice_fusion.11
  153.7 0.9 slice_dynamic-update-slice_fusion.10
  154.7 0.9 slice_dynamic-update-slice_fusion.9
  156.6 1.0 slice_dynamic-update-slice_fusion.7
  157.5 1.0 slice_dynamic-update-slice_fusion.6
  158.5 0.9 slice_dynamic-update-slice_fusion.5
  159.5 1.0 slice_dynamic-update-slice_fusion.4
  160.4 0.9 slice_dynamic-update-slice_fusion.3
  161.4 0.9 slice_dynamic-update-slice_fusion.2
  162.3 0.9 slice_dynamic-update-slice_fusion.1
  164.3 1.7 fusion.41
  166.9 3.4 %multiply_reduce_fusion = (f32[512]{0:T(512)S(1)}, f32[512,2048]{1,0:T(8,128)}) fusion(bf16[512,2048]{1,0:T(8,128)(2,1)S(1)} %slice_dynamic-update-slice_fusion, bf16[512,256]{1,0:T(8,128)(2,1)S(1)} %bitcast.160, bf16[512,256]{1,0:T(8,128)(2,1)S(1)} %bitcast.158, bf16[512,2048]{1,0:T(8,128)(2,1)S(1)} %slice_dynamic-update-slice_fusion.16), kind=kOutput, calls=%fused_computation.1 | convolution fusion | flops 1078984192 | bytes 8914944 | tf_op jit(solution)/shard_map/dot_general | solution.py:171
  170.3 7.4 %convolution_convert_fusion.1 = bf16[512,1408]{1,0:T(8,128)(2,1)S(1)} fusion(bf16[2048,1408]{1,0:T(8,128)(2,1)} %bitcast.179, f32[512,2048]{1,0:T(8,128)} %get-tuple-element.64, f32[2048]{0:T(1024)S(1)} %constant_dynamic-update-slice_fusion.1, f32[512]{0:T(512)S(1)} %add_rsqrt_fusion), kind=kOutput, calls=%fused_computation.4 | convolution fusion | flops 2956656640 | bytes 11413504 | tf_op jit(solution)/shard_map/dot_general | solution.py:176
  177.7 1.1 copy-done.3
  179.9 4.0 %copy.74 = bf16[704,4,4,128]{3,2,1,0:T(4,128)(2,1)S(1)} copy(bf16[704,4,4,128]{3,0,1,2:T(8,128)(2,1)} %bitcast.157) | data formatting | bytes 5767168 | tf_op jit(solution)/shard_map/transpose | solution.py:134
  183.9 3.4 %reshape.293 = bf16[704,2048]{1,0:T(8,128)(2,1)} reshape(bf16[704,4,4,128]{3,2,1,0:T(4,128)(2,1)S(1)} %copy.74) | data formatting | bytes 5767168 | tf_op jit(solution)/shard_map/reshape | solution.py:134
  187.3 1.7 maximum_convert_fusion
  190.4 1.3 copy-done.1
  191.7 1.8 convolution_convert_fusion
  193.7 1.5 pad_maximum_fusion
  195.3 70.3 %reduce-scatter.2.cloned.1.call-done = bf16[1,128,1024]{2,1,0:T(8,128)(2,1)} async-done(((bf16[8,128,1024]{2,1,0:T(8,128)(2,1)}), bf16[1,128,1024]{2,1,0:T(8,128)(2,1)}) %reduce-scatter.2.cloned.1.call-update) | async-done | bytes 262160 | tf_op jit(solution)/shard_map/reduce_scatter | solution.py:207
  265.6 2.0 fusion.6
  (155 shorter events, 27.7 us)
Async XLA Ops:
  6.5 2.9 %copy-start.5 = (bf16[128,2816]{1,0:T(8,128)(2,1)S(1)}, bf16[128,2816]{1,0:T(8,128)(2,1)}, u32[]{:S(2)}) copy-start(bf16[128,2816]{1,0:T(8,128)(2,1)} %param.24) | copy-start | bytes 2162692
  6.5 142.4 %all-gather.13.cloned.1.call-start = ((), (), s32[]{:S(2)}) async-start(), calls=%async_computation.5 | async-start | bytes 3145728 | tf_op jit(solution)/shard_map/all_gather | solution.py:136
  7.3 157.0 %all-gather.11.cloned.1.call-start = ((), (), s32[]{:S(2)}) async-start(), calls=%async_computation.4 | async-start | bytes 2359296 | tf_op jit(solution)/shard_map/all_gather | solution.py:105
  8.0 162.3 %all-gather.15.cloned.1.call-start = ((), (), s32[]{:S(2)}) async-start(), calls=%async_computation.6 | async-start | bytes 7208960 | tf_op jit(solution)/shard_map/all_gather | solution.py:102
  50.8 3.8 %copy-start.6 = (bf16[128,256]{1,0:T(8,128)(2,1)S(1)}, bf16[128,256]{1,0:T(8,128)(2,1)}, u32[]{:S(2)}) copy-start(bf16[128,256]{1,0:T(8,128)(2,1)} %param.16) | copy-start | bytes 196612
  50.8 3.8 %copy-start.10 = (f32[256]{0:T(256)S(1)}, f32[256]{0:T(256)}, u32[]{:S(2)}) copy-start(f32[256]{0:T(256)} %param.19) | copy-start | bytes 3076
  50.8 4.9 %copy-start.7 = (bf16[128,256]{1,0:T(8,128)(2,1)S(1)}, bf16[128,256]{1,0:T(8,128)(2,1)}, u32[]{:S(2)}) copy-start(bf16[128,256]{1,0:T(8,128)(2,1)} %param.15) | copy-start | bytes 196612
  50.8 5.1 %copy-start.8 = (bf16[128,256]{1,0:T(8,128)(2,1)S(1)}, bf16[128,256]{1,0:T(8,128)(2,1)}, u32[]{:S(2)}) copy-start(bf16[128,256]{1,0:T(8,128)(2,1)} %param.17) | copy-start | bytes 196612
  50.8 97.0 %all-to-all-start.1 = ((bf16[4,704,128]{2,1,0:T(8,128)(2,1)}), bf16[4,704,128]{2,1,0:T(8,128)(2,1)S(1)}, u32[]{:S(2)}, u32[]{:S(2)}) async-start(bf16[4,704,128]{2,1,0:T(8,128)(2,1)} %bitcast.45), calls=%async_computation.1 | async-start | bytes 1441792 | tf_op jit(solution)/shard_map/all_to_all | solution.py:97
  54.5 125.4 %all-gather.17.cloned.1.call-start = ((), (), s32[]{:S(2)}) async-start(), calls=%async_computation.7 | async-start | bytes 3604480 | tf_op jit(solution)/shard_map/all_gather | solution.py:102
  108.7 1.9 copy-start.11
  108.7 2.1 copy-start.9
  108.7 6.5 %copy-start.12 = (f32[2048]{0:T(1024)S(1)}, f32[2048]{0:T(1024)}, u32[]{:S(2)}) copy-start(f32[2048]{0:T(1024)} %custom-call) | copy-start | bytes 24580
  147.8 0.9 copy-start.2
  148.7 116.8 %reduce-scatter.2.cloned.1.call-start = ((), (), s32[]{:S(2)}) async-start(), calls=%async_computation.3 | async-start | bytes 2359296 | tf_op jit(solution)/shard_map/reduce_scatter | solution.py:207
  177.7 1.1 copy-start.3
  178.8 8.4 %collective-permute-start = (bf16[4,2,1408]{2,1,0:T(2,128)(2,1)S(1)}, bf16[4,2,1408]{2,1,0:T(2,128)(2,1)S(1)}, u32[]{:S(2)}, u32[]{:S(2)}) collective-permute-start(bf16[4,2,1408]{2,1,0:T(2,128)(2,1)S(1)} %slice.628), channel_id=1, source_target_pairs={{0,2},{2,4},{4,6},{6,0},{8,10},{10,12},{12,14},{14,8},{16,18},{18,... | collective-permute-start | bytes 67592 | tf_op jit(solution)/shard_map/ppermute | solution.py:184
  189.9 1.8 copy-start.1
  195.2 70.3 %copy-start = (bf16[512,1024]{1,0:T(8,128)(2,1)S(1)}, bf16[512,1024]{1,0:T(8,128)(2,1)}, u32[]{:S(2)}) copy-start(bf16[512,1024]{1,0:T(8,128)(2,1)} %param.21) | copy-start | bytes 3145732
  195.2 70.3 %copy-start.4 = (bf16[128,1024]{1,0:T(8,128)(2,1)S(1)}, bf16[128,1024]{1,0:T(8,128)(2,1)}, u32[]{:S(2)}) copy-start(bf16[128,1024]{1,0:T(8,128)(2,1)} %param.14) | copy-start | bytes 786436
Sparse Core Ops, SparseCore 0:
  8.9 35.8 all-gather.12
  46.8 59.2 all-gather.10
  107.8 41.8 all-gather.14
  151.1 27.0 all-gather.16
  195.4 70.1 reduce-scatter.1

commit v3 on v2

--- a/solution.py
+++ b/solution.py
@@ -167,6 +167,7 @@
     gating = jax.nn.silu(gate_pre.astype(f32)).reshape(recurrent.shape)
     head_out = (scaled * gating).reshape(rows, heads * DK).astype(bf16)
 
+    head_out, out_full = lax.optimization_barrier((head_out, out_full))
     head_group = jnp.concatenate(gather_wide(head_out), axis=1)
     stream = residual_group.astype(f32) + jnp.dot(
         head_group, out_full, preferred_element_type=f32
@@ -197,19 +198,10 @@
     terms = jnp.dot(
         hidden.reshape(outer * rows, chunk), down_chunk, preferred_element_type=f32
     ).astype(bf16)
-    terms = jnp.stack(
-        [
-            terms[:, t * my_width : (t + 1) * my_width].reshape(outer, rows, my_width)
-            for t in range(tp)
-        ],
-        axis=1,
-    )
     summed = lax.psum_scatter(
-        terms.reshape(outer * tp, rows, my_width),
-        ("sp", "tp"),
-        scatter_dimension=0,
-        axis_index_groups=wide_groups,
-    )
+        terms, "sp", scatter_dimension=0, tiled=True, axis_index_groups=outer_groups
+    )
+    summed = lax.psum_scatter(summed, "tp", scatter_dimension=1, tiled=True)
     my_heads = lax.dynamic_slice_in_dim(head_group, my_outer * rows, rows, axis=0)
     own = residual_in.astype(f32) + jnp.dot(
         my_heads, out_weight, preferred_element_type=f32

time: 275 us -> 263 us (0.956)
  local copies, waits for them, and re-layouts: 45.2 us -> 35.9 us
    reduce_scatter x1 -> x2, waiting for transfers between devices: 70.3 us -> 59.7 us  [the longest x1 43.7 us: on_device(): lax.psum_scatter(terms, 'sp', scatter_dimension=0, tiled=True, axis_index...]
    all_gather x2, waiting for transfers between devices: 0.02 us -> 8.49 us  [gather_inner(): return lax.all_gather(array, 'sp', axis_index_groups=inner_groups)]
    mul x14, local copies, waits for them, and re-layouts: 9.1 us -> 1.14 us  [on_device(): advanced = entering * decays[j] + everyone[j, :DK]]
    unnamed x73 -> x71, local copies, waits for them, and re-layouts: 18.4 us -> 18.5 us
  transfers between devices with their start and end apart: 7 -> 8, of which waited for: 1 -> 3; matrix products, arithmetic and copies ran while one was open for 22% -> 19% of each run, Pallas kernels for 0% -> 0%
where the time goes in v3:
time: 263 us; the launch traced here: 262 us
  blocking collectives  113 us (43%)
  waiting for transfers between devices  69.7 us (27%)
  local copies, waits for them, and re-layouts  35.9 us (14%)
  matrix products  19.2 us (7%)
  between operations  14.4 us (5%)
  other arithmetic  5.76 us (2%)
  starting transfers between devices  3.9 us (1%)
    reduce_scatter x1, waiting for transfers between devices, on_device(): lax.psum_scatter(terms, 'sp', scatter_dimension=0, tiled=True, axis_index...  43.7 us
    all_to_all x1, blocking collectives, exchange(): lax.all_to_all(array, 'sp', 0, 0, axis_index_groups=outer_groups, tiled=T...  40.4 us
    all_gather x1, blocking collectives, on_device(): everyone = lax.all_gather(packed, 'sp').astype(f32)  35.8 us
    all_gather x1, blocking collectives, gather_wide(): lax.all_gather(array, ('sp', 'tp'), axis_index_groups=wide_groups)  32.7 us
    unnamed x71, local copies, waits for them, and re-layouts  18.5 us
    reduce_scatter x1, waiting for transfers between devices, on_device(): summed = lax.psum_scatter(summed, 'tp', scatter_dimension=1, tiled=True)  15.9 us
    all_gather x2, waiting for transfers between devices, gather_inner(): return lax.all_gather(array, 'sp', axis_index_groups=inner_groups)  8.49 us
    dot_general x1, matrix products, on_device(): up = jnp.dot(normed, up_chunk, preferred_element_type=f32).astype(bf16)  7.36 us
  transfers between devices with their start and end apart: 8, of which 3 were waited for; matrix products, arithmetic and copies ran while one was open for 19% of the time, Pallas kernels for 0%

profile of v3, /device:TPU:0, one launch (start us, length us, event | category | flops | bytes accessed | tf_op | source)
XLA Modules:
  0.0 262.0 jit_solution(9370654994997921655)
XLA Ops:
  8.1 1.4 fusion.41
  10.4 40.4 %all_to_all.10 = bf16[4,128,1408]{2,1,0:T(8,128)(2,1)} all-to-all(bf16[4,128,1408]{2,1,0:T(8,128)(2,1)S(1)} %pad_maximum_fusion), channel_id=1, replica_groups={{0,8,16,24},{2,10,18,26},{4,12,20,28},{6,14,22,30},{1,9,17,25},{3,11,19..., dimensions={0} | all-to-all | bytes 2883584 | tf_op jit(solution)/shard_map/all_to_all | solution.py:97
  50.8 3.6 %all-to-all-start.1 = ((bf16[4,704,128]{2,1,0:T(8,128)(2,1)}), bf16[4,704,128]{2,1,0:T(8,128)(2,1)S(1)}, u32[]{:S(2)}, u32[]{:S(2)}) async-start(bf16[4,704,128]{2,1,0:T(8,128)(2,1)} %bitcast.45), calls=%async_computation.1 | async-start | bytes 1441792 | tf_op jit(solution)/shard_map/all_to_all | solution.py:97
  56.6 35.8 %all-gather = bf16[1280,256]{1,0:T(8,128)(2,1)S(1)} all-gather(bf16[80,256]{1,0:T(8,128)(2,1)S(1)} %concatenate.36), channel_id=2, replica_groups=mesh['grp'=1,'sp'=16,'tp'=2] {'sp'}, dimensions={0}, use_global_device_ids=true | all-gather | bytes 696320 | tf_op jit(solution)/shard_map/all_gather | solution.py:152
  92.9 4.4 %all-gather.4 = f32[2048]{0:T(1024)S(1)} all-gather(f32[1024]{0:T(1024)S(1)} %copy-done.9), channel_id=6, replica_groups=mesh['grp'=1,'sp'=16,'tp'=2] {'tp'}, dimensions={0}, use_global_device_ids=true | all-gather | bytes 12288 | tf_op jit(solution)/shard_map/all_gather | solution.py:137
  98.5 2.1 fusion.8
  108.1 0.9 slice_dynamic-update-slice_fusion.29
  109.1 0.9 slice_dynamic-update-slice_fusion.28
  110.0 0.9 slice_dynamic-update-slice_fusion.27
  111.0 0.9 slice_dynamic-update-slice_fusion.26
  111.9 1.0 slice_dynamic-update-slice_fusion.25
  112.9 1.0 slice_dynamic-update-slice_fusion.24
  113.9 1.0 slice_dynamic-update-slice_fusion.23
  114.9 0.9 slice_dynamic-update-slice_fusion.22
  115.8 1.0 slice_dynamic-update-slice_fusion.21
  116.8 1.0 slice_dynamic-update-slice_fusion.20
  117.8 0.9 slice_dynamic-update-slice_fusion.19
  118.7 0.9 slice_dynamic-update-slice_fusion.18
  121.7 32.7 %all-gather.2 = bf16[1024,256]{1,0:T(8,128)(2,1)S(1)} all-gather(bf16[128,256]{1,0:T(8,128)(2,1)S(1)} %copy.65), channel_id=4, replica_groups={{0,1,8,9,16,17,24,25},{2,3,10,11,18,19,26,27},{4,5,12,13,20,21,28,29},{..., dimensions={0}, use_global_device_ids=true | all-gather | bytes 589824 | tf_op jit(solution)/shard_map/all_gather | solution.py:105
  154.4 1.7 fusion.40
  157.1 3.4 %multiply_reduce_fusion = (f32[512]{0:T(512)S(1)}, f32[512,2048]{1,0:T(8,128)}) fusion(bf16[512,2048]{1,0:T(8,128)(2,1)S(1)} %slice_dynamic-update-slice_fusion.16, bf16[512,256]{1,0:T(8,128)(2,1)S(1)} %bitcast.147, bf16[512,256]{1,0:T(8,128)(2,1)S(1)} %bitcast.145, bf16[512,2048]{1,0:T(8,128)(2,1)S(1)} %slice_dynamic-update-slice_fusion), kind=kOutput, calls=%fused_computation.1 | convolution fusion | flops 1078984192 | bytes 8914944 | tf_op jit(solution)/shard_map/dot_general | solution.py:172
  160.5 7.4 %convolution_convert_fusion.1 = bf16[512,1408]{1,0:T(8,128)(2,1)S(1)} fusion(bf16[2048,1408]{1,0:T(8,128)(2,1)} %bitcast.166, f32[512,2048]{1,0:T(8,128)} %get-tuple-element.66, f32[2048]{0:T(1024)S(1)} %constant_dynamic-update-slice_fusion.1, f32[512]{0:T(512)S(1)} %add_rsqrt_fusion), kind=kOutput, calls=%fused_computation.4 | convolution fusion | flops 2956656640 | bytes 11413504 | tf_op jit(solution)/shard_map/dot_general | solution.py:177
  167.8 1.1 copy-done.3
  170.0 8.5 %all-gather.18.cloned.1.call-done = bf16[16,704,128]{2,1,0:T(8,128)(2,1)} async-done(((bf16[4,704,128]{2,1,0:T(8,128)(2,1)}), bf16[16,704,128]{2,1,0:T(8,128)(2,1)}) %all-gather.18.cloned.1.call-update) | async-done | bytes 2883600 | tf_op jit(solution)/shard_map/all_gather | solution.py:102
  178.5 4.0 %copy.68 = bf16[704,4,4,128]{3,2,1,0:T(4,128)(2,1)S(1)} copy(bf16[704,4,4,128]{3,0,1,2:T(8,128)(2,1)} %bitcast.144) | data formatting | bytes 5767168 | tf_op jit(solution)/shard_map/transpose | solution.py:134
  182.5 3.4 %reshape.278 = bf16[704,2048]{1,0:T(8,128)(2,1)} reshape(bf16[704,4,4,128]{3,2,1,0:T(4,128)(2,1)S(1)} %copy.68) | data formatting | bytes 5767168 | tf_op jit(solution)/shard_map/reshape | solution.py:134
  185.9 1.7 maximum_convert_fusion
  189.0 1.3 copy-done.1
  190.3 3.1 %convolution_convert_fusion = bf16[512,2048]{1,0:T(8,128)(2,1)} fusion(bf16[512,704]{1,0:T(8,128)(2,1)S(1)} %bitcast.153, bf16[704,2048]{1,0:T(8,128)(2,1)S(1)} %copy-done.1), kind=kOutput, calls=%fused_computation.3 | convolution fusion | flops 1477443584 | bytes 5701632 | tf_op jit(solution)/shard_map/dot_general | solution.py:198
  193.5 43.7 %reduce-scatter.3.cloned.1.call-done = bf16[128,2048]{1,0:T(8,128)(2,1)} async-done(((bf16[512,2048]{1,0:T(8,128)(2,1)}), bf16[128,2048]{1,0:T(8,128)(2,1)}) %reduce-scatter.3.cloned.1.call-update) | async-done | bytes 524304 | tf_op jit(solution)/shard_map/reduce_scatter | solution.py:201
  237.3 15.9 %reduce-scatter.5.cloned.1.call-done = bf16[128,1024]{1,0:T(8,128)(2,1)} async-done(((bf16[128,2048]{1,0:T(8,128)(2,1)}), bf16[128,1024]{1,0:T(8,128)(2,1)}) %reduce-scatter.5.cloned.1.call-update) | async-done | bytes 262160 | tf_op jit(solution)/shard_map/reduce_scatter | solution.py:204
  253.2 2.0 fusion.6
  (154 shorter events, 18.6 us)
Async XLA Ops:
  6.5 2.9 %copy-start.5 = (bf16[128,2816]{1,0:T(8,128)(2,1)S(1)}, bf16[128,2816]{1,0:T(8,128)(2,1)}, u32[]{:S(2)}) copy-start(bf16[128,2816]{1,0:T(8,128)(2,1)} %param.24) | copy-start | bytes 2162692
  6.5 99.7 %all-gather.12.cloned.1.call-start = ((), (), s32[]{:S(2)}) async-start(), calls=%async_computation.6 | async-start | bytes 3145728 | tf_op jit(solution)/shard_map/all_gather | solution.py:136
  7.3 147.2 %all-gather.14.cloned.1.call-start = ((), (), s32[]{:S(2)}) async-start(), calls=%async_computation.7 | async-start | bytes 2359296 | tf_op jit(solution)/shard_map/all_gather | solution.py:105
  8.0 152.5 %all-gather.16.cloned.1.call-start = ((), (), s32[]{:S(2)}) async-start(), calls=%async_computation.8 | async-start | bytes 7208960 | tf_op jit(solution)/shard_map/all_gather | solution.py:102
  50.8 3.8 %copy-start.6 = (bf16[128,256]{1,0:T(8,128)(2,1)S(1)}, bf16[128,256]{1,0:T(8,128)(2,1)}, u32[]{:S(2)}) copy-start(bf16[128,256]{1,0:T(8,128)(2,1)} %param.16) | copy-start | bytes 196612
  50.8 3.8 %copy-start.10 = (f32[256]{0:T(256)S(1)}, f32[256]{0:T(256)}, u32[]{:S(2)}) copy-start(f32[256]{0:T(256)} %param.19) | copy-start | bytes 3076
  50.8 4.9 %copy-start.7 = (bf16[128,256]{1,0:T(8,128)(2,1)S(1)}, bf16[128,256]{1,0:T(8,128)(2,1)}, u32[]{:S(2)}) copy-start(bf16[128,256]{1,0:T(8,128)(2,1)} %param.15) | copy-start | bytes 196612
  50.8 5.1 %copy-start.8 = (bf16[128,256]{1,0:T(8,128)(2,1)S(1)}, bf16[128,256]{1,0:T(8,128)(2,1)}, u32[]{:S(2)}) copy-start(bf16[128,256]{1,0:T(8,128)(2,1)} %param.17) | copy-start | bytes 196612
  50.8 54.5 %all-to-all-start.1 = ((bf16[4,704,128]{2,1,0:T(8,128)(2,1)}), bf16[4,704,128]{2,1,0:T(8,128)(2,1)S(1)}, u32[]{:S(2)}, u32[]{:S(2)}) async-start(bf16[4,704,128]{2,1,0:T(8,128)(2,1)} %bitcast.45), calls=%async_computation.1 | async-start | bytes 1441792 | tf_op jit(solution)/shard_map/all_to_all | solution.py:97
  54.5 124.0 %all-gather.18.cloned.1.call-start = ((), (), s32[]{:S(2)}) async-start(), calls=%async_computation.9 | async-start | bytes 3604480 | tf_op jit(solution)/shard_map/all_gather | solution.py:102
  55.8 37.1 %copy-start.9 = (f32[1024]{0:T(1024)S(1)}, f32[1024]{0:T(1024)}, u32[]{:S(2)}) copy-start(f32[1024]{0:T(1024)} %param.22) | copy-start | bytes 12292
  103.6 1.6 copy-start.11
  105.3 0.9 copy-start.2
  106.2 131.1 %reduce-scatter.3.cloned.1.call-start = ((), (), s32[]{:S(2)}) async-start(), calls=%async_computation.4 | async-start | bytes 2621440 | tf_op jit(solution)/shard_map/reduce_scatter | solution.py:201
  167.8 1.1 copy-start.3
  169.0 16.9 %collective-permute-start = (bf16[4,2,1408]{2,1,0:T(2,128)(2,1)S(1)}, bf16[4,2,1408]{2,1,0:T(2,128)(2,1)S(1)}, u32[]{:S(2)}, u32[]{:S(2)}) collective-permute-start(bf16[4,2,1408]{2,1,0:T(2,128)(2,1)S(1)} %slice.620), channel_id=1, source_target_pairs={{0,2},{2,4},{4,6},{6,0},{8,10},{10,12},{12,14},{14,8},{16,18},{18,... | collective-permute-start | bytes 67592 | tf_op jit(solution)/shard_map/ppermute | solution.py:185
  188.5 1.8 copy-start.1
  193.4 59.8 %copy-start = (bf16[512,1024]{1,0:T(8,128)(2,1)S(1)}, bf16[512,1024]{1,0:T(8,128)(2,1)}, u32[]{:S(2)}) copy-start(bf16[512,1024]{1,0:T(8,128)(2,1)} %param.21) | copy-start | bytes 3145732
  193.4 59.8 %copy-start.4 = (bf16[128,1024]{1,0:T(8,128)(2,1)S(1)}, bf16[128,1024]{1,0:T(8,128)(2,1)}, u32[]{:S(2)}) copy-start(bf16[128,1024]{1,0:T(8,128)(2,1)} %param.14) | copy-start | bytes 786436
  193.5 59.8 %reduce-scatter.5.cloned.1.call-start = ((), (), s32[]{:S(2)}) async-start(), calls=%async_computation.5 | async-start | bytes 786432 | tf_op jit(solution)/shard_map/reduce_scatter | solution.py:204
Sparse Core Ops, SparseCore 0:
  8.9 35.8 all-gather.11
  46.8 59.1 all-gather.13
  107.6 42.0 all-gather.15
  151.2 27.2 all-gather.17
  193.6 43.6 reduce-scatter.2
  239.3 13.8 reduce-scatter.4
